TPU v7x, 32 devices: a whole 2x2x4 slice. The times are simulated.
32 devices in a mesh: ep: 8 (over z, x), tp: 4 (over y, core).
Axes of the slice: x: 2, y: 2, z: 4, core: 2. Of those that a mesh axis runs over, the one named last changes fastest.
Arguments:
- hidden_in: bfloat16 [128, 4096], P('ep'), may hold values from -6 to 6
- w_query: bfloat16 [4096, 2048], P('ep', 'tp'), may hold values from -0.09375 to 0.09375
- w_key: bfloat16 [4096, 2048], P('ep', 'tp'), may hold values from -0.09375 to 0.09375
- w_value: bfloat16 [4096, 2048], P('ep', 'tp'), may hold values from -0.09375 to 0.09375
- w_outgate: bfloat16 [4096, 2048], P('ep', 'tp'), may hold values from -0.09375 to 0.09375
- w_igate: bfloat16 [4096, 16], P('ep', 'tp'), may hold values from -0.09375 to 0.09375
- w_fgate: bfloat16 [4096, 16], P('ep', 'tp'), may hold values from -0.09375 to 0.09375
- input_bias: float32 [16], P('tp'), may hold values from -3 to 303
- forget_bias: float32 [16], P('tp'), may hold values from -1 to 5
- mem_state: float32 [128, 16, 16384], P('ep', 'tp'), may hold values from -4 to 4
- max_state: float32 [128, 16], P('ep', 'tp'), may hold values from -4 to 304
- head_gain: float32 [2048], P('tp'), may hold values from 0.1 to 1.9
- w_output: bfloat16 [2048, 4096], P('tp'), may hold values from -0.26367188 to 0.26367188
- first_gain: float32 [4096], replicated, may hold values from 0.35 to 3.25
- w_group_router: bfloat16 [4096, 2], replicated, may hold values from -0.09375 to 0.09375
- w_expert_router: bfloat16 [4096, 8], replicated, may hold values from -0.09375 to 0.09375
- expert_route: int32 [128, 2], P('ep'), may hold values from 0 to 7, as said below
- w_expgate: bfloat16 [8, 4096, 1024], P('ep', None, 'tp'), may hold values from -0.09375 to 0.09375
- w_expup: bfloat16 [8, 4096, 1024], P('ep', None, 'tp'), may hold values from -0.09375 to 0.09375
- w_expdown: bfloat16 [8, 1024, 4096], P('ep', 'tp'), may hold values from -0.75 to 0.75
- second_gain: float32 [4096], P('tp'), may hold values from 0.1 to 1.9
Outputs:
- hidden_out: bfloat16 [128, 4096], P('ep', 'tp')
- mem_next: float32 [128, 16, 16384], P('ep', 'tp')
- max_next: float32 [128, 16], P('ep', 'tp')
Inputs may be any that keep to these rules, and one draw needn't show every extreme that they name: `expert_route`: each row names two different experts of one group (an expert's group is its number divided by 4). In each aligned block of 16 rows (the rows of one index of ep) every group is named by exactly 8 rows, no expert by more than 8 rows, and some expert by exactly 8 rows.
All inputs are finite; a program needn't handle non-finite values.
Results may differ from a plain program's by a relative error of at most 0.02.
Values may be sent and summed in bfloat16 or wider, within the bound.
A program may use at most 64 MiB of HBM per device.

v0:
```python
import functools

import jax
import jax.numpy as jnp
from jax import lax
from jax.experimental import pallas as pl
from jax.experimental.pallas import tpu as pltpu
from jax.sharding import PartitionSpec as P

D = 4096
DH = 128
GROUP_SIZE = 4
MESH = pl.DeviceIdType.MESH


res_alpha = 8.0**0.25


def layer_norm(values, gain):
    row_mean = jnp.mean(values, -1, keepdims=True)
    row_var = jnp.mean(values * values, -1, keepdims=True) - row_mean * row_mean
    return (values - row_mean) * lax.rsqrt(row_var + 1e-05) * gain


def mlstm_step(queries, keys_scaled, values, log_input, log_forget, memory, stabilizer):
    new_max = jnp.maximum(log_forget + stabilizer, log_input)
    keep_old = jnp.exp(log_forget + stabilizer - new_max)
    write_new = jnp.exp(log_input - new_max)
    scores = jnp.sum(queries * keys_scaled, -1) * write_new
    read_old = jnp.einsum("bhd,bhde->bhe", queries, memory, precision=lax.Precision.HIGHEST)
    readout = scores[..., None] * values + keep_old[..., None] * read_old
    memory_next = (
        keep_old[..., None, None] * memory
        + write_new[..., None, None] * keys_scaled[..., :, None] * values[..., None, :]
    )
    return (readout, memory_next, new_max)


def head_mix(readout, head_gain, out_pre):
    scaled = readout * lax.rsqrt(jnp.mean(readout * readout, -1, keepdims=True) + 1e-06)
    flat_heads = scaled.reshape(scaled.shape[0], -1)
    return (flat_heads * head_gain * jax.nn.sigmoid(out_pre)).astype(jnp.bfloat16)


def route_weights(mid_float, w_group_router, w_expert_router, expert_route):
    group_logits = jnp.dot(
        mid_float, w_group_router.astype(jnp.float32), precision=lax.Precision.HIGHEST
    )
    expert_logits = jnp.dot(
        mid_float, w_expert_router.astype(jnp.float32), precision=lax.Precision.HIGHEST
    )
    first_expert = expert_route[:, 0]
    second_expert = expert_route[:, 1]
    expert_ids = lax.broadcasted_iota(jnp.int32, expert_logits.shape, 1)
    group_ids = lax.broadcasted_iota(jnp.int32, group_logits.shape, 1)
    first_logit = jnp.sum(jnp.where(expert_ids == first_expert[:, None], expert_logits, 0.0), -1)
    second_logit = jnp.sum(jnp.where(expert_ids == second_expert[:, None], expert_logits, 0.0), -1)
    group_pick = jnp.sum(
        jnp.where(group_ids == (first_expert // GROUP_SIZE)[:, None], group_logits, 0.0), -1
    )
    group_gate = jax.nn.sigmoid(group_pick)
    return (
        group_gate * jax.nn.sigmoid(first_logit - second_logit),
        group_gate * jax.nn.sigmoid(second_logit - first_logit),
    )


def slot_ranks(flat_routes, expert_total):
    onehot = (
        flat_routes[:, None]
        == lax.broadcasted_iota(jnp.int32, (flat_routes.shape[0], expert_total), 1)
    ).astype(jnp.int32)
    running = jnp.cumsum(onehot, 0)
    return jnp.sum((running - 1) * onehot, -1)


def body(
    hidden_in,
    w_query,
    w_key,
    w_value,
    w_outgate,
    w_igate,
    w_fgate,
    input_bias,
    forget_bias,
    mem_state,
    max_state,
    head_gain,
    w_output,
    first_gain,
    w_group_router,
    w_expert_router,
    expert_route,
    w_expgate,
    w_expup,
    w_expdown,
    second_gain,
):
    own_rows, width = hidden_in.shape
    heads_here = mem_state.shape[1]
    head_width = heads_here * DH
    top_count = expert_route.shape[1]
    spread_rows = lax.all_to_all(hidden_in, "ep", split_axis=1, concat_axis=0, tiled=True)
    stacked_w = jnp.concatenate([w_query, w_key, w_value, w_outgate], 1)
    gate_w = jnp.concatenate([w_igate, w_fgate], 1)
    proj_terms = jnp.dot(spread_rows, stacked_w, preferred_element_type=jnp.float32)
    gate_terms = jnp.dot(spread_rows, gate_w, preferred_element_type=jnp.float32)
    projected, gate_sums = (
        lax.psum_scatter(proj_terms, "ep", scatter_dimension=0, tiled=True),
        lax.psum_scatter(gate_terms, "ep", scatter_dimension=0, tiled=True),
    )
    shaped = projected.reshape(own_rows, 4, heads_here, DH)
    queries = shaped[:, 0]
    keys_raw = shaped[:, 1]
    values = shaped[:, 2]
    out_pre = shaped[:, 3].reshape(own_rows, head_width)
    input_sum = gate_sums[:, :heads_here]
    forget_sum = gate_sums[:, heads_here:]
    keys_scaled = keys_raw * DH ** (-0.5)
    log_input = input_sum + input_bias
    log_forget = jax.nn.log_sigmoid(forget_sum + forget_bias)
    memory = mem_state.reshape(own_rows, heads_here, DH, DH)
    readout, memory_square, new_max = mlstm_step(
        queries, keys_scaled, values, log_input, log_forget, memory, max_state
    )
    memory_next = memory_square.reshape(own_rows, heads_here, DH * DH)
    mixed_heads = head_mix(readout, head_gain, out_pre)
    partial_mix = jnp.dot(mixed_heads, w_output, preferred_element_type=jnp.float32).astype(
        jnp.bfloat16
    )
    mix = lax.psum(partial_mix.astype(jnp.float32).astype(jnp.bfloat16), "tp").astype(jnp.float32)
    mid_float = layer_norm(res_alpha * hidden_in.astype(jnp.float32) + mix, first_gain)
    mid = mid_float.astype(jnp.bfloat16)
    first_weight, second_weight = route_weights(
        mid_float, w_group_router, w_expert_router, expert_route
    )
    expert_total = w_expgate.shape[0] * lax.axis_size("ep")
    capacity = 2 * own_rows * top_count // expert_total
    flat_routes = expert_route.reshape(-1)
    local_slot = flat_routes * capacity + slot_ranks(flat_routes, expert_total)
    share_width = width // lax.axis_size("tp")
    mid_share = lax.dynamic_slice_in_dim(mid, lax.axis_index("tp") * share_width, share_width, 1)
    buffer = (
        jnp.zeros((expert_total * capacity, width), jnp.bfloat16)
        .at[local_slot]
        .set(jnp.repeat(mid, top_count, 0))
    )
    arrived = lax.all_to_all(
        buffer.reshape(expert_total, capacity, width), "ep", split_axis=0, concat_axis=1, tiled=True
    )
    gate_pre = jnp.einsum("erd,edf->erf", arrived, w_expgate, preferred_element_type=jnp.float32)
    up_pre = jnp.einsum("erd,edf->erf", arrived, w_expup, preferred_element_type=jnp.float32)
    hidden_units = (jax.nn.silu(gate_pre) * up_pre).astype(jnp.bfloat16)
    down_terms = jnp.einsum(
        "erf,efd->erd", hidden_units, w_expdown, preferred_element_type=jnp.float32
    ).astype(jnp.bfloat16)
    expert_share = lax.psum_scatter(
        down_terms.astype(jnp.float32).astype(jnp.bfloat16), "tp", scatter_dimension=2, tiled=True
    )
    returned = lax.all_to_all(expert_share, "ep", split_axis=1, concat_axis=0, tiled=True)
    picked = returned.reshape(expert_total * capacity, share_width)[local_slot]
    picked = picked.astype(jnp.float32).reshape(own_rows, top_count, share_width)
    moe = first_weight[:, None] * picked[:, 0] + second_weight[:, None] * picked[:, 1]
    joined = res_alpha * mid_share.astype(jnp.float32) + moe
    row_sum, square_sum = lax.psum((jnp.sum(joined, -1), jnp.sum(joined * joined, -1)), "tp")
    row_mean = row_sum / D
    row_var = square_sum / D - row_mean * row_mean
    hidden_out = (
        (joined - row_mean[:, None]) * lax.rsqrt(row_var[:, None] + 1e-05) * second_gain
    ).astype(jnp.bfloat16)
    return (hidden_out, memory_next, new_max)


def greet(peers):
    barrier = pltpu.get_barrier_semaphore()
    for peer in peers:
        pl.semaphore_signal(barrier, inc=1, device_id=peer, device_id_type=MESH)
    pl.semaphore_wait(barrier, len(peers))


def remote(source, target, send_sem, recv_sem, peer):
    return pltpu.make_async_remote_copy(
        src_ref=source,
        dst_ref=target,
        send_sem=send_sem,
        recv_sem=recv_sem,
        device_id=peer,
        device_id_type=MESH,
    )


def project_kernel(
    n_ep,
    hidden,
    gate_w,
    wq,
    wk,
    wv,
    wo,
    proj_out,
    gate_out,
    weights,
    spread,
    send_buf,
    recv_buf,
    gate_send,
    gate_recv,
    load_sem,
    h_send,
    h_recv,
    p_send,
    p_recv,
    g_send,
    g_recv,
):
    me = lax.axis_index("ep")
    tp = lax.axis_index("tp")
    rows = hidden.shape[0]
    depth, cols = wq.shape
    loads = [pltpu.make_async_copy(w, weights.at[i], load_sem.at[i]) for i, w in enumerate((wq, wk, wv, wo))]
    for load in loads:
        load.start()
    after = [(lax.rem(me + o, n_ep), tp) for o in range(n_ep)]
    before = [(lax.rem(me + n_ep - o, n_ep), tp) for o in range(n_ep)]
    greet(after[1:])
    sent = []
    for o in range(1, n_ep):
        columns = pl.ds(pl.multiple_of(after[o][0] * depth, depth), depth)
        copy = remote(hidden.at[:, columns], spread.at[o], h_send.at[o], h_recv.at[o], after[o])
        copy.start()
        sent.append(copy)
    spread[0] = hidden[:, pl.ds(pl.multiple_of(me * depth, depth), depth)]
    for load in loads:
        load.wait()
    for copy in sent:
        copy.wait_recv()
    lhs = spread[...].reshape(n_ep * rows, depth)
    gates = jnp.dot(lhs, gate_w[...], preferred_element_type=jnp.float32)
    gate_send[...] = gates.reshape(n_ep, rows, gates.shape[1])
    for i in range(4):
        part = jnp.dot(lhs, weights[i], preferred_element_type=jnp.float32)
        send_buf[:, :, i * cols : (i + 1) * cols] = part.astype(jnp.bfloat16).reshape(n_ep, rows, cols)
    back = []
    for o in range(1, n_ep):
        back.append(remote(gate_send.at[o], gate_recv.at[o], g_send.at[o], g_recv.at[o], before[o]))
        back.append(remote(send_buf.at[o], recv_buf.at[o], p_send.at[o], p_recv.at[o], before[o]))
    for copy in back:
        copy.start()
    gate_total = gate_send[0]
    proj_out[...] = send_buf[0].astype(jnp.float32)
    for o in range(1, n_ep):
        back[2 * o - 2].wait_recv()
        back[2 * o - 1].wait_recv()
        gate_total += gate_recv[o]
        proj_out[...] += recv_buf[o].astype(jnp.float32)
    gate_out[...] = gate_total
    for copy in sent + back:
        copy.wait_send()


def project(n_ep, hidden, gate_w, wq, wk, wv, wo):
    rows = hidden.shape[0]
    depth, cols = wq.shape
    vmem = pl.BlockSpec(memory_space=pltpu.VMEM)
    anywhere = pl.BlockSpec(memory_space=pl.ANY)
    sems = pltpu.SemaphoreType.DMA((n_ep,))
    return pl.pallas_call(
        functools.partial(project_kernel, n_ep),
        out_shape=(
            jax.ShapeDtypeStruct((rows, 4 * cols), jnp.float32),
            jax.ShapeDtypeStruct((rows, gate_w.shape[1]), jnp.float32),
        ),
        in_specs=[vmem, vmem] + [anywhere] * 4,
        out_specs=(vmem, vmem),
        scratch_shapes=[
            pltpu.VMEM((4, depth, cols), jnp.bfloat16),
            pltpu.VMEM((n_ep, rows, depth), jnp.bfloat16),
            pltpu.VMEM((n_ep, rows, 4 * cols), jnp.bfloat16),
            pltpu.VMEM((n_ep, rows, 4 * cols), jnp.bfloat16),
            pltpu.VMEM((n_ep, rows, gate_w.shape[1]), jnp.float32),
            pltpu.VMEM((n_ep, rows, gate_w.shape[1]), jnp.float32),
            pltpu.SemaphoreType.DMA((4,)),
        ]
        + [sems] * 6,
        compiler_params=pltpu.CompilerParams(collective_id=0, has_side_effects=True),
        name="project",
    )(hidden, gate_w, wq, wk, wv, wo)


def cell_kernel(proj, keep_ref, write_ref, gain_ref, mem_ref, mixed_ref, mem_out):
    heads = mem_ref.shape[1]
    queries = proj[0, 0:heads]
    keys = proj[0, heads : 2 * heads] * DH ** (-0.5)
    values = proj[0, 2 * heads : 3 * heads]
    out_pre = proj[0, 3 * heads : 4 * heads]
    keep = keep_ref[0]
    write = write_ref[0]
    write_keys = keys * write
    read_old = jnp.zeros_like(queries)
    for d in range(DH):
        block = mem_ref[0, :, d * DH : (d + 1) * DH]
        read_old += queries[:, d : d + 1] * block
        mem_out[0, :, d * DH : (d + 1) * DH] = keep * block + write_keys[:, d : d + 1] * values
    scores = jnp.sum(queries * keys, -1, keepdims=True) * write
    readout = scores * values + keep * read_old
    scaled = readout * lax.rsqrt(jnp.mean(readout * readout, -1, keepdims=True) + 1e-06)
    mixed_ref[0] = (scaled * gain_ref[...] * jax.nn.sigmoid(out_pre)).astype(jnp.bfloat16)


def cell(proj, keep, write, gain, memory):
    rows, heads, flat = memory.shape
    one = lambda *dims: pl.BlockSpec((1,) + dims, lambda b: (b,) + (0,) * len(dims))
    return pl.pallas_call(
        cell_kernel,
        grid=(rows,),
        out_shape=(
            jax.ShapeDtypeStruct((rows, heads, DH), jnp.bfloat16),
            jax.ShapeDtypeStruct((rows, heads, flat), jnp.float32),
        ),
        in_specs=[
            one(4 * heads, DH),
            one(heads, DH),
            one(heads, DH),
            pl.BlockSpec((heads, DH), lambda b: (0, 0)),
            one(heads, flat),
        ],
        out_specs=(one(heads, DH), one(heads, flat)),
        name="cell",
    )(proj, keep, write, gain, memory)


def moe_kernel(
    n_ep,
    n_tp,
    groups,
    mixed,
    hidden,
    gain1,
    gain2,
    router_t,
    route,
    perm,
    perm_t,
    w_out,
    w_gate,
    w_up,
    w_down,
    out_ref,
    wo_buf,
    wg_buf,
    wu_buf,
    wd_buf,
    mix_send,
    mix_recv,
    mid_buf,
    arrived,
    down_send,
    down_recv,
    ret_send,
    ret_recv,
    stat_send,
    stat_recv,
    load_sem,
    m_send,
    m_recv,
    a_send,
    a_recv,
    d_send,
    d_recv,
    r_send,
    r_recv,
    s_send,
    s_recv,
):
    me = lax.axis_index("ep")
    tp = lax.axis_index("tp")
    rows, width = hidden.shape
    share = width // n_tp
    block = rows // groups
    loads = [
        pltpu.make_async_copy(w_out, wo_buf, load_sem.at[0]),
        pltpu.make_async_copy(w_gate.at[0], wg_buf, load_sem.at[1]),
        pltpu.make_async_copy(w_up.at[0], wu_buf, load_sem.at[2]),
        pltpu.make_async_copy(w_down.at[0], wd_buf, load_sem.at[3]),
    ]
    for load in loads:
        load.start()
    ep_after = [(lax.rem(me + o, n_ep), tp) for o in range(n_ep)]
    ep_before = [(lax.rem(me + n_ep - o, n_ep), tp) for o in range(n_ep)]
    tp_after = [(me, lax.rem(tp + o, n_tp)) for o in range(n_tp)]
    greet(ep_after[1:] + tp_after[1:])
    started = []

    def begin(copies):
        for copy in copies:
            copy.start()
        started.extend(copies)
        return copies

    mixed_sorted = jnp.dot(perm[...], mixed[...], preferred_element_type=jnp.float32).astype(jnp.bfloat16)
    loads[0].wait()
    for c in range(n_tp):
        columns = slice(c * share, (c + 1) * share)
        mix_send[:, columns] = jnp.dot(
            mixed_sorted, wo_buf[:, columns], preferred_element_type=jnp.float32
        ).astype(jnp.bfloat16)
    copies = begin(
        [remote(mix_send, mix_recv.at[o], m_send.at[o], m_recv.at[o], tp_after[o]) for o in range(1, n_tp)]
    )
    joined = res_alpha * jnp.dot(perm[...], hidden[...], preferred_element_type=jnp.float32)
    joined += mix_send[...].astype(jnp.float32)
    for o in range(1, n_tp):
        copies[o - 1].wait_recv()
        joined += mix_recv[o].astype(jnp.float32)
    mid_float = layer_norm(joined, gain1[...])
    for g in range(groups):
        mid_buf[g] = mid_float[g * block : (g + 1) * block].astype(jnp.bfloat16)
    copies = begin(
        [
            remote(
                mid_buf.at[lax.div(ep_after[o][0], GROUP_SIZE)],
                arrived.at[o],
                a_send.at[o],
                a_recv.at[o],
                ep_after[o],
            )
            for o in range(1, n_ep)
        ]
    )
    high = mid_float.astype(jnp.bfloat16)
    rest = mid_float - high.astype(jnp.float32)
    middle = rest.astype(jnp.bfloat16)
    low = (rest - middle.astype(jnp.float32)).astype(jnp.bfloat16)
    logits = jnp.zeros((rows, router_t.shape[0]), jnp.float32)
    for piece in (low, middle, high):
        logits += lax.dot_general(
            piece, router_t[...], (((1,), (1,)), ((), ())), preferred_element_type=jnp.float32
        )
    first = route[:, 0:1]
    second = route[:, 1:2]
    lanes = lax.broadcasted_iota(jnp.int32, logits.shape, 1)
    pick = lambda index: jnp.sum(jnp.where(lanes == index, logits, 0.0), -1, keepdims=True)
    first_logit = pick(first)
    second_logit = pick(second)
    group_gate = jax.nn.sigmoid(pick(n_ep + lax.shift_right_logical(first, 2)))
    weight1 = group_gate * jax.nn.sigmoid(first_logit - second_logit)
    weight2 = group_gate * jax.nn.sigmoid(second_logit - first_logit)
    arrived[0] = mid_buf[lax.div(me, GROUP_SIZE)]
    loads[1].wait()
    loads[2].wait()
    for copy in copies:
        copy.wait_recv()
    tokens = arrived[...].astype(jnp.float32).reshape(n_ep * block, width).astype(jnp.bfloat16)
    gate_pre = jnp.dot(tokens, wg_buf[...], preferred_element_type=jnp.float32)
    up_pre = jnp.dot(tokens, wu_buf[...], preferred_element_type=jnp.float32)
    units = (gate_pre * jax.nn.sigmoid(gate_pre) * up_pre).astype(jnp.bfloat16)
    loads[3].wait()
    copies = []
    for o in list(range(1, n_tp)) + [0]:
        columns = pl.ds(pl.multiple_of(tp_after[o][1] * share, share), share)
        down_send[o] = jnp.dot(units, wd_buf[:, columns], preferred_element_type=jnp.float32).astype(
            jnp.bfloat16
        )
        if o:
            copies += begin(
                [remote(down_send.at[o], down_recv.at[o], d_send.at[o], d_recv.at[o], tp_after[o])]
            )
    total = down_send[0].astype(jnp.float32)
    for o in range(1, n_tp):
        copies[o - 1].wait_recv()
        total += down_recv[o].astype(jnp.float32)
    for o in range(n_ep):
        ret_send[o] = total[o * block : (o + 1) * block].astype(jnp.bfloat16)
    copies = begin(
        [
            remote(ret_send.at[o], ret_recv.at[o], r_send.at[o], r_recv.at[o], ep_before[o])
            for o in range(1, n_ep)
        ]
    )
    mine = pl.ds(pl.multiple_of(tp * share, share), share)
    joined = res_alpha * mid_buf[:, :, mine].astype(jnp.float32).reshape(rows, share)
    for o in range(n_ep):
        expert = ep_after[o][0]
        if o:
            copies[o - 1].wait_recv()
        result = (ret_recv[o] if o else ret_send[0]).astype(jnp.float32)
        weight = jnp.where(first == expert, weight1, 0.0) + jnp.where(second == expert, weight2, 0.0)
        joined += weight * jnp.concatenate([result] * groups, 0)
    row_sum = jnp.sum(joined, -1, keepdims=True)
    square_sum = jnp.sum(joined * joined, -1, keepdims=True)
    stat_send[0] = jnp.broadcast_to(row_sum, stat_send.shape[1:])
    stat_send[1] = jnp.broadcast_to(square_sum, stat_send.shape[1:])
    copies = begin(
        [remote(stat_send, stat_recv.at[o], s_send.at[o], s_recv.at[o], tp_after[o]) for o in range(1, n_tp)]
    )
    for o in range(1, n_tp):
        copies[o - 1].wait_recv()
        row_sum += stat_recv[o, 0][:, 0:1]
        square_sum += stat_recv[o, 1][:, 0:1]
    row_mean = row_sum / width
    row_var = square_sum / width - row_mean * row_mean
    result = ((joined - row_mean) * lax.rsqrt(row_var + 1e-05) * gain2[...]).astype(jnp.bfloat16)
    out_ref[...] = jnp.dot(perm_t[...], result, preferred_element_type=jnp.float32).astype(jnp.bfloat16)
    for copy in started:
        copy.wait_send()


def mix_and_moe(n_ep, n_tp, groups, *operands):
    mixed, hidden = operands[:2]
    w_out, w_gate, w_up, w_down = operands[-4:]
    rows, width = hidden.shape
    share = width // n_tp
    block = rows // groups
    vmem = pl.BlockSpec(memory_space=pltpu.VMEM)
    anywhere = pl.BlockSpec(memory_space=pl.ANY)
    ep_sems = pltpu.SemaphoreType.DMA((n_ep,))
    tp_sems = pltpu.SemaphoreType.DMA((n_tp,))
    half = jnp.bfloat16
    return pl.pallas_call(
        functools.partial(moe_kernel, n_ep, n_tp, groups),
        out_shape=jax.ShapeDtypeStruct((rows, share), half),
        in_specs=[vmem] * (len(operands) - 4) + [anywhere] * 4,
        out_specs=vmem,
        scratch_shapes=[
            pltpu.VMEM(w_out.shape, half),
            pltpu.VMEM(w_gate.shape[1:], half),
            pltpu.VMEM(w_up.shape[1:], half),
            pltpu.VMEM(w_down.shape[1:], half),
            pltpu.VMEM((rows, width), half),
            pltpu.VMEM((n_tp, rows, width), half),
            pltpu.VMEM((groups, block, width), half),
            pltpu.VMEM((n_ep, block, width), half),
            pltpu.VMEM((n_tp, n_ep * block, share), half),
            pltpu.VMEM((n_tp, n_ep * block, share), half),
            pltpu.VMEM((n_ep, block, share), half),
            pltpu.VMEM((n_ep, block, share), half),
            pltpu.VMEM((2, rows, DH), jnp.float32),
            pltpu.VMEM((n_tp, 2, rows, DH), jnp.float32),
            pltpu.SemaphoreType.DMA((4,)),
            tp_sems,
            tp_sems,
            ep_sems,
            ep_sems,
            tp_sems,
            tp_sems,
            ep_sems,
            ep_sems,
            tp_sems,
            tp_sems,
        ],
        compiler_params=pltpu.CompilerParams(collective_id=1, has_side_effects=True),
        name="mix_and_moe",
    )(*operands)


def kernel_body(
    hidden_in,
    w_query,
    w_key,
    w_value,
    w_outgate,
    w_igate,
    w_fgate,
    input_bias,
    forget_bias,
    mem_state,
    max_state,
    head_gain,
    w_output,
    first_gain,
    w_group_router,
    w_expert_router,
    expert_route,
    w_expgate,
    w_expup,
    w_expdown,
    second_gain,
):
    n_ep, n_tp = lax.axis_size("ep"), lax.axis_size("tp")
    rows, width = hidden_in.shape
    heads = mem_state.shape[1]
    groups = w_group_router.shape[1]
    gate_w = jnp.concatenate([w_igate, w_fgate], 1)
    gate_w = jnp.pad(gate_w, ((0, 0), (0, DH - 2 * heads)))
    projected, gate_sums = project(n_ep, hidden_in, gate_w, w_query, w_key, w_value, w_outgate)
    log_input = gate_sums[:, :heads] + input_bias
    log_forget = jax.nn.log_sigmoid(gate_sums[:, heads : 2 * heads] + forget_bias)
    new_max = jnp.maximum(log_forget + max_state, log_input)
    keep_old = jnp.exp(log_forget + max_state - new_max)
    write_new = jnp.exp(log_input - new_max)
    spread_gate = lambda gate: jnp.broadcast_to(gate[:, :, None], (rows, heads, DH))
    mixed, memory_next = cell(
        projected.reshape(rows, 4 * heads, DH),
        spread_gate(keep_old),
        spread_gate(write_new),
        head_gain.reshape(heads, DH),
        mem_state,
    )
    row_ids = jnp.arange(rows, dtype=jnp.int32)
    group = expert_route[:, 0] // GROUP_SIZE
    earlier = (group[:, None] == group[None, :]) & (row_ids[None, :] < row_ids[:, None])
    place = group * (rows // groups) + jnp.sum(earlier.astype(jnp.int32), 1)
    perm = place[None, :] == row_ids[:, None]
    route = jnp.sum(jnp.where(perm[:, :, None], expert_route[None], 0), 1)
    router = jnp.concatenate([w_expert_router, w_group_router], 1)
    router_t = jnp.pad(router, ((0, 0), (0, -router.shape[1] % 16))).T
    hidden_out = mix_and_moe(
        n_ep,
        n_tp,
        groups,
        mixed.reshape(rows, heads * DH),
        hidden_in,
        first_gain[None],
        second_gain[None],
        router_t,
        route,
        perm.astype(jnp.bfloat16),
        perm.T.astype(jnp.bfloat16),
        w_output,
        w_expgate,
        w_expup,
        w_expdown,
    )
    return (hidden_out, memory_next, new_max)


def either_body(*operands):
    hidden_in, w_query, group_router, experts = operands[0], operands[1], operands[14], operands[17]
    rows, width = hidden_in.shape
    block, odd_rows = divmod(rows, group_router.shape[1])
    aligned = rows % 16 == 0 and block % 8 == 0 and odd_rows == 0 and experts.shape[0] == 1
    aligned = aligned and w_query.shape[0] % DH == 0 and width // lax.axis_size("tp") % DH == 0
    return (kernel_body if aligned else body)(*operands)


def solution(mesh):
    return jax.shard_map(
        either_body,
        mesh=mesh,
        in_specs=(
            P("ep", None),
            P("ep", "tp"),
            P("ep", "tp"),
            P("ep", "tp"),
            P("ep", "tp"),
            P("ep", "tp"),
            P("ep", "tp"),
            P("tp"),
            P("tp"),
            P("ep", "tp", None),
            P("ep", "tp"),
            P("tp"),
            P("tp", None),
            P(),
            P(),
            P(),
            P("ep", None),
            P("ep", None, "tp"),
            P("ep", None, "tp"),
            P("ep", "tp", None),
            P("tp"),
        ),
        out_specs=(P("ep", "tp"), P("ep", "tp", None), P("ep", "tp")),
        check_vma=False,
    )
```

profile of v0, /device:TPU:0, one launch (start us, length us, event | category | flops | bytes accessed | tf_op | source)
XLA Modules:
  0.0 95.0 jit_solution(17866947812730903020)
XLA Ops:
  0.6 0.0 copy-start.2
  0.6 0.0 copy-start.1
  0.7 0.0 copy-start
  0.7 0.7 pad_maximum_fusion
  1.4 0.2 copy.33
  1.6 0.7 pad.8.gate_w
  2.3 27.0 %project.1 = (f32[16,2048]{1,0:T(8,128)}, f32[16,128]{1,0:T(8,128)}) custom-call(bf16[16,4096]{1,0:T(8,128)(2,1)} %hidden.3, bf16[512,128]{1,0:T(8,128)(2,1)} %pad.8.gate_w, bf16[512,512]{1,0:T(8,128)(2,1)} %wq.1, bf16[512,512]{1,0:T(8,128)(2,1)} %wk.1, bf16[512,512]{1,0:T(8,128)(2,1)} %wv.1, bf16[512,512]{1,0:T(8,128)(2,1)} %wo.1), custom_call_target="tpu_custom_call" | custom-call | tf_op jit(solution)/shard_map/project/pallas_call | solution.py:268
  29.2 0.8 copy.34
  30.0 0.9 subtract_exponential_fusion
  30.9 0.8 subtract_exponential_fusion.1
  31.7 0.7 broadcast_in_dim.21.keep_ref
  32.4 0.7 broadcast_in_dim.22.write_ref
  33.1 1.6 %copy.37 = f32[2,8,16,128]{3,2,1,0:T(8,128)} copy(f32[2,8,16,128]{3,1,2,0:T(8,128)} %bitcast.24) | data formatting | bytes 262144
  34.7 14.7 %cell.1 = (bf16[16,4,128]{2,1,0:T(4,128)(2,1)}, f32[16,4,16384]{2,1,0:T(4,128)}) custom-call(f32[16,16,128]{2,1,0:T(8,128)} %bitcast.23, f32[16,4,128]{2,1,0:T(4,128)} %broadcast_in_dim.21.keep_ref, f32[16,4,128]{2,1,0:T(4,128)} %broadcast_in_dim.22.write_ref, f32[4,128]{1,0:T(4,128)} %bitcast.29, f32[16,4,16384]{2,1,0:T(4,128)} %mem_ref.1), custom_call_target="tpu_custom_call" | custom-call | tf_op jit(solution)/shard_map/cell/pallas_call | solution.py:314
  49.3 1.3 %copy.40 = bf16[2,8,4,128]{3,1,2,0:T(8,128)(2,1)} copy(bf16[2,8,4,128]{3,2,1,0:T(4,128)(2,1)} %bitcast.27) | data formatting | bytes 32768
  50.7 0.0 copy-done.2
  50.7 0.2 convert_reduce_fusion
  50.9 0.7 fusion.7
  51.6 0.1 select_reduce_fusion
  51.7 0.7 copy.35.route
  52.4 0.0 copy-done.1
  52.4 0.0 copy-done
  52.4 0.7 fusion.3.router_t
  53.0 39.9 %mix_and_moe.1 = bf16[16,1024]{1,0:T(8,128)(2,1)} custom-call(bf16[16,512]{1,0:T(8,128)(2,1)} %bitcast.25, bf16[16,4096]{1,0:T(8,128)(2,1)} %hidden.3, f32[1,4096]{1,0:T(1,128)} %bitcast.26, f32[1,1024]{1,0:T(1,128)} %bitcast.28, bf16[16,4096]{1,0:T(8,128)(2,1)} %fusion.3.router_t, s32[16,2]{1,0:T(8,128)} %copy.35.route, ...), custom_call_target="tpu_custom_call" | custom-call | tf_op jit(solution)/shard_map/mix_and_moe/pallas_call | solution.py:520
  92.9 0.7 copy.36
  93.6 1.4 %copy.42 = bf16[16,1024]{1,0:T(8,128)(2,1)} copy(bf16[16,1024]{1,0:T(8,128)(2,1)} %mix_and_moe.1) | data formatting | bytes 65536
  (3 shorter events, 0.0 us)
Async XLA Ops:
  0.6 50.0 %copy-start.2 = (s32[16,2]{0,1:T(2,128)S(1)}, s32[16,2]{0,1:T(2,128)}, u32[]{:S(2)}) copy-start(s32[16,2]{0,1:T(2,128)} %param.37) | copy-start | bytes 388
  0.6 51.7 %copy-start.1 = (bf16[4096,2]{0,1:T(2,128)(2,1)S(1)}, bf16[4096,2]{0,1:T(2,128)(2,1)}, u32[]{:S(2)}) copy-start(bf16[4096,2]{0,1:T(2,128)(2,1)} %param.35) | copy-start | bytes 49156
  0.7 51.7 %copy-start = (bf16[4096,8]{0,1:T(8,128)(2,1)S(1)}, bf16[4096,8]{0,1:T(8,128)(2,1)}, u32[]{:S(2)}) copy-start(bf16[4096,8]{0,1:T(8,128)(2,1)} %param.36) | copy-start | bytes 196612
where the time goes:
time: 95.7 us; the launch traced here: 95 us
  Pallas kernels  81.6 us (85%)
  local copies, waits for them, and re-layouts  8.61 us (9%)
  other arithmetic  4.08 us (4%)
    pallas_call x1, Pallas kernels, mix_and_moe(): pl.pallas_call(functools.partial(moe_kernel, n_ep, n_tp, groups), out_sha...  39.9 us
    pallas_call x1, Pallas kernels, project(): pl.pallas_call(functools.partial(project_kernel, n_ep), out_shape=(jax.Sh...  27 us
    pallas_call x1, Pallas kernels, cell(): pl.pallas_call(cell_kernel, grid=(rows,), out_shape=(jax.ShapeDtypeStruct...  14.7 us
    unnamed x11, local copies, waits for them, and re-layouts  5.7 us

commit v1 on v0

v1 whole, which is shorter than its diff:
```python
import functools

import jax
import jax.numpy as jnp
from jax import lax
from jax.experimental import pallas as pl
from jax.experimental.pallas import tpu as pltpu
from jax.sharding import PartitionSpec as P

D = 4096
DH = 128
GROUP_SIZE = 4
MESH = pl.DeviceIdType.MESH


res_alpha = 8.0**0.25


def layer_norm(values, gain):
    row_mean = jnp.mean(values, -1, keepdims=True)
    row_var = jnp.mean(values * values, -1, keepdims=True) - row_mean * row_mean
    return (values - row_mean) * lax.rsqrt(row_var + 1e-05) * gain


def mlstm_step(queries, keys_scaled, values, log_input, log_forget, memory, stabilizer):
    new_max = jnp.maximum(log_forget + stabilizer, log_input)
    keep_old = jnp.exp(log_forget + stabilizer - new_max)
    write_new = jnp.exp(log_input - new_max)
    scores = jnp.sum(queries * keys_scaled, -1) * write_new
    read_old = jnp.einsum("bhd,bhde->bhe", queries, memory, precision=lax.Precision.HIGHEST)
    readout = scores[..., None] * values + keep_old[..., None] * read_old
    memory_next = (
        keep_old[..., None, None] * memory
        + write_new[..., None, None] * keys_scaled[..., :, None] * values[..., None, :]
    )
    return (readout, memory_next, new_max)


def head_mix(readout, head_gain, out_pre):
    scaled = readout * lax.rsqrt(jnp.mean(readout * readout, -1, keepdims=True) + 1e-06)
    flat_heads = scaled.reshape(scaled.shape[0], -1)
    return (flat_heads * head_gain * jax.nn.sigmoid(out_pre)).astype(jnp.bfloat16)


def route_weights(mid_float, w_group_router, w_expert_router, expert_route):
    group_logits = jnp.dot(
        mid_float, w_group_router.astype(jnp.float32), precision=lax.Precision.HIGHEST
    )
    expert_logits = jnp.dot(
        mid_float, w_expert_router.astype(jnp.float32), precision=lax.Precision.HIGHEST
    )
    first_expert = expert_route[:, 0]
    second_expert = expert_route[:, 1]
    expert_ids = lax.broadcasted_iota(jnp.int32, expert_logits.shape, 1)
    group_ids = lax.broadcasted_iota(jnp.int32, group_logits.shape, 1)
    first_logit = jnp.sum(jnp.where(expert_ids == first_expert[:, None], expert_logits, 0.0), -1)
    second_logit = jnp.sum(jnp.where(expert_ids == second_expert[:, None], expert_logits, 0.0), -1)
    group_pick = jnp.sum(
        jnp.where(group_ids == (first_expert // GROUP_SIZE)[:, None], group_logits, 0.0), -1
    )
    group_gate = jax.nn.sigmoid(group_pick)
    return (
        group_gate * jax.nn.sigmoid(first_logit - second_logit),
        group_gate * jax.nn.sigmoid(second_logit - first_logit),
    )


def slot_ranks(flat_routes, expert_total):
    onehot = (
        flat_routes[:, None]
        == lax.broadcasted_iota(jnp.int32, (flat_routes.shape[0], expert_total), 1)
    ).astype(jnp.int32)
    running = jnp.cumsum(onehot, 0)
    return jnp.sum((running - 1) * onehot, -1)


def body(
    hidden_in,
    w_query,
    w_key,
    w_value,
    w_outgate,
    w_igate,
    w_fgate,
    input_bias,
    forget_bias,
    mem_state,
    max_state,
    head_gain,
    w_output,
    first_gain,
    w_group_router,
    w_expert_router,
    expert_route,
    w_expgate,
    w_expup,
    w_expdown,
    second_gain,
):
    own_rows, width = hidden_in.shape
    heads_here = mem_state.shape[1]
    head_width = heads_here * DH
    top_count = expert_route.shape[1]
    spread_rows = lax.all_to_all(hidden_in, "ep", split_axis=1, concat_axis=0, tiled=True)
    stacked_w = jnp.concatenate([w_query, w_key, w_value, w_outgate], 1)
    gate_w = jnp.concatenate([w_igate, w_fgate], 1)
    proj_terms = jnp.dot(spread_rows, stacked_w, preferred_element_type=jnp.float32)
    gate_terms = jnp.dot(spread_rows, gate_w, preferred_element_type=jnp.float32)
    projected, gate_sums = (
        lax.psum_scatter(proj_terms, "ep", scatter_dimension=0, tiled=True),
        lax.psum_scatter(gate_terms, "ep", scatter_dimension=0, tiled=True),
    )
    shaped = projected.reshape(own_rows, 4, heads_here, DH)
    queries = shaped[:, 0]
    keys_raw = shaped[:, 1]
    values = shaped[:, 2]
    out_pre = shaped[:, 3].reshape(own_rows, head_width)
    input_sum = gate_sums[:, :heads_here]
    forget_sum = gate_sums[:, heads_here:]
    keys_scaled = keys_raw * DH ** (-0.5)
    log_input = input_sum + input_bias
    log_forget = jax.nn.log_sigmoid(forget_sum + forget_bias)
    memory = mem_state.reshape(own_rows, heads_here, DH, DH)
    readout, memory_square, new_max = mlstm_step(
        queries, keys_scaled, values, log_input, log_forget, memory, max_state
    )
    memory_next = memory_square.reshape(own_rows, heads_here, DH * DH)
    mixed_heads = head_mix(readout, head_gain, out_pre)
    partial_mix = jnp.dot(mixed_heads, w_output, preferred_element_type=jnp.float32).astype(
        jnp.bfloat16
    )
    mix = lax.psum(partial_mix.astype(jnp.float32).astype(jnp.bfloat16), "tp").astype(jnp.float32)
    mid_float = layer_norm(res_alpha * hidden_in.astype(jnp.float32) + mix, first_gain)
    mid = mid_float.astype(jnp.bfloat16)
    first_weight, second_weight = route_weights(
        mid_float, w_group_router, w_expert_router, expert_route
    )
    expert_total = w_expgate.shape[0] * lax.axis_size("ep")
    capacity = 2 * own_rows * top_count // expert_total
    flat_routes = expert_route.reshape(-1)
    local_slot = flat_routes * capacity + slot_ranks(flat_routes, expert_total)
    share_width = width // lax.axis_size("tp")
    mid_share = lax.dynamic_slice_in_dim(mid, lax.axis_index("tp") * share_width, share_width, 1)
    buffer = (
        jnp.zeros((expert_total * capacity, width), jnp.bfloat16)
        .at[local_slot]
        .set(jnp.repeat(mid, top_count, 0))
    )
    arrived = lax.all_to_all(
        buffer.reshape(expert_total, capacity, width), "ep", split_axis=0, concat_axis=1, tiled=True
    )
    gate_pre = jnp.einsum("erd,edf->erf", arrived, w_expgate, preferred_element_type=jnp.float32)
    up_pre = jnp.einsum("erd,edf->erf", arrived, w_expup, preferred_element_type=jnp.float32)
    hidden_units = (jax.nn.silu(gate_pre) * up_pre).astype(jnp.bfloat16)
    down_terms = jnp.einsum(
        "erf,efd->erd", hidden_units, w_expdown, preferred_element_type=jnp.float32
    ).astype(jnp.bfloat16)
    expert_share = lax.psum_scatter(
        down_terms.astype(jnp.float32).astype(jnp.bfloat16), "tp", scatter_dimension=2, tiled=True
    )
    returned = lax.all_to_all(expert_share, "ep", split_axis=1, concat_axis=0, tiled=True)
    picked = returned.reshape(expert_total * capacity, share_width)[local_slot]
    picked = picked.astype(jnp.float32).reshape(own_rows, top_count, share_width)
    moe = first_weight[:, None] * picked[:, 0] + second_weight[:, None] * picked[:, 1]
    joined = res_alpha * mid_share.astype(jnp.float32) + moe
    row_sum, square_sum = lax.psum((jnp.sum(joined, -1), jnp.sum(joined * joined, -1)), "tp")
    row_mean = row_sum / D
    row_var = square_sum / D - row_mean * row_mean
    hidden_out = (
        (joined - row_mean[:, None]) * lax.rsqrt(row_var[:, None] + 1e-05) * second_gain
    ).astype(jnp.bfloat16)
    return (hidden_out, memory_next, new_max)


VMEM_LIMIT = 59 * 1024 * 1024


def announce(peers):
    barrier = pltpu.get_barrier_semaphore()
    for peer in peers:
        pl.semaphore_signal(barrier, inc=1, device_id=peer, device_id_type=MESH)
    return barrier


def remote(source, target, send_sem, recv_sem, peer):
    return pltpu.make_async_remote_copy(
        src_ref=source,
        dst_ref=target,
        send_sem=send_sem,
        recv_sem=recv_sem,
        device_id=peer,
        device_id_type=MESH,
    )


def flip(index, bits):
    result = index
    place = 1
    while place <= bits:
        if bits & place:
            result = result + place * (1 - 2 * lax.rem(lax.div(index, place), 2))
        place *= 2
    return result


def three_parts(value):
    high = value.astype(jnp.bfloat16).astype(jnp.float32)
    rest = value - high
    middle = rest.astype(jnp.bfloat16).astype(jnp.float32)
    return high, middle, rest - middle


def dot32(left, right):
    return jnp.dot(left, right, preferred_element_type=jnp.float32)


def dot_t(left, right):
    return lax.dot_general(left, right, (((1,), (1,)), ((), ())), preferred_element_type=jnp.float32)


def layer_kernel(
    n_ep,
    n_tp,
    groups,
    hidden_hbm,
    wq,
    wk,
    wv,
    wo,
    memory,
    w_out,
    w_gate,
    w_up,
    w_down,
    w_igate_t_hbm,
    w_fgate_t_hbm,
    input_bias_hbm,
    forget_bias_hbm,
    max_state_t_hbm,
    head_gain_hbm,
    gain1_hbm,
    gain2_hbm,
    group_router_t_hbm,
    expert_router_t_hbm,
    route_t_hbm,
    out_ref,
    mem_out,
    max_out,
    w_igate_t,
    w_fgate_t,
    input_bias,
    forget_bias,
    max_state_t,
    head_gain,
    gain1,
    gain2,
    group_router_t,
    expert_router_t,
    route_t,
    hid,
    weights,
    wo_buf,
    wg_buf,
    wu_buf,
    wd_buf,
    mem_half,
    gate_w,
    spread,
    proj_send,
    proj_recv,
    proj_own,
    far_own,
    far_recv,
    cross_send,
    cross_recv,
    cross_send2,
    cross_recv2,
    write_keys,
    keep_buf,
    value_buf,
    mix_send,
    mix_recv,
    sum_send,
    sum_recv,
    row_send,
    arrived,
    arrived2,
    stat_send,
    stat_recv,
    weight_buf,
    mid_buf,
    down_send,
    down_recv,
    ret_send,
    ret_recv,
    stat2_send,
    stat2_recv,
    load_sem,
    small_sem,
    h_send,
    h_recv,
    p_send,
    p_recv,
    f_send,
    f_recv,
    c_send,
    c_recv,
    m_send,
    m_recv,
    u_send,
    u_recv,
    a_send,
    a_recv,
    b_send,
    b_recv,
    s_send,
    s_recv,
    d_send,
    d_recv,
    r_send,
    r_recv,
    t_send,
    t_recv,
):
    me = lax.axis_index("ep")
    tp = lax.axis_index("tp")
    n_y = n_tp // 2
    y = lax.div(tp, 2)
    core = lax.rem(tp, 2)
    rows, width = hid.shape
    share = width // n_tp
    block = rows // groups
    heads = keep_buf.shape[0]
    depth, cols = wq.shape
    far_first = list(range(n_ep - 1, 0, -1))
    near_first = list(range(1, n_ep))
    ep_peer = [flip(me, k) for k in range(n_ep)]
    y_peer = [lax.rem(y + j, n_y) for j in range(n_y)]
    y_from = [lax.rem(y + n_y - j, n_y) for j in range(n_y)]
    tp_peer = [lax.rem(tp + o, n_tp) for o in range(n_tp)]
    partner = (me, 2 * y + 1 - core)
    started = []

    def begin(copy):
        copy.start()
        started.append(copy)
        return copy

    def share_of(index):
        return pl.ds(pl.multiple_of(index * share, share), share)

    peers = [(ep_peer[k], tp) for k in range(1, n_ep)]
    peers += [(me, tp_peer[o]) for o in range(1, n_tp)]
    peers += [(ep_peer[k], 2 * y_peer[j] + core) for k in range(1, n_ep) for j in range(1, n_y)]
    barrier = announce(peers)
    hidden_load = pltpu.make_async_copy(hidden_hbm, hid, load_sem.at[0])
    hidden_load.start()
    small_loads = [
        pltpu.make_async_copy(source, target, small_sem.at[i])
        for i, (source, target) in enumerate(
            (
                (w_igate_t_hbm, w_igate_t),
                (w_fgate_t_hbm, w_fgate_t),
                (input_bias_hbm, input_bias),
                (forget_bias_hbm, forget_bias),
                (max_state_t_hbm, max_state_t),
                (head_gain_hbm, head_gain),
                (gain1_hbm, gain1),
                (gain2_hbm, gain2),
                (group_router_t_hbm, group_router_t),
                (expert_router_t_hbm, expert_router_t),
                (route_t_hbm, route_t),
            )
        )
    ]
    w_loads = [pltpu.make_async_copy(w, weights.at[i], load_sem.at[1 + i]) for i, w in enumerate((wq, wk, wv, wo))]
    mem_load = pltpu.make_async_copy(memory, mem_out, load_sem.at[5])
    out_load = pltpu.make_async_copy(w_out, wo_buf, load_sem.at[6])
    gate_load = pltpu.make_async_copy(w_gate.at[0], wg_buf, load_sem.at[7])
    up_load = pltpu.make_async_copy(w_up.at[0], wu_buf, load_sem.at[8])
    down_load = pltpu.make_async_copy(w_down.at[0], wd_buf, load_sem.at[9])
    for load in small_loads + w_loads + [mem_load, out_load, gate_load, up_load, down_load]:
        load.start()
    hidden_load.wait()
    pl.semaphore_wait(barrier, len(peers))

    spreads = {}
    for k in far_first:
        columns = pl.ds(pl.multiple_of(ep_peer[k] * depth, depth), depth)
        spreads[k] = begin(remote(hid.at[:, columns], spread.at[k], h_send.at[k], h_recv.at[k], (ep_peer[k], tp)))
    spread[0] = hid[:, pl.ds(pl.multiple_of(me * depth, depth), depth)]
    for load in small_loads:
        load.wait()
    gate_w[...] = jnp.zeros_like(gate_w)
    in_rows = w_igate_t[...].astype(jnp.float32)
    forget_rows = w_fgate_t[...].astype(jnp.float32)
    for part in range(3):
        gate_w[2 * heads * part : 2 * heads * part + heads] = in_rows
        gate_w[2 * heads * part + heads : 2 * heads * (part + 1)] = forget_rows
    gate_half = gate_w[...].astype(jnp.bfloat16)

    mem_load.wait()

    def convert(b, carry):
        for h in range(heads):
            mem_half[h, pl.ds(pl.multiple_of(b * DH, DH), DH), :] = mem_out[b, pl.ds(h, DH, stride=heads), :].astype(
                jnp.bfloat16
            )
        return carry

    lax.fori_loop(0, rows, convert, 0)
    i_row = lax.broadcasted_iota(jnp.int32, (rows, rows), 0)
    i_col = lax.broadcasted_iota(jnp.int32, (rows, rows), 1)
    eye = i_row == i_col
    spread_row = lambda row: jnp.broadcast_to(row, (rows, rows))
    to_column = lambda row: jnp.sum(jnp.where(eye, spread_row(row), 0.0), 1, keepdims=True)
    to_row = lambda column: jnp.sum(jnp.where(eye, jnp.broadcast_to(column, (rows, rows)), 0.0), 0, keepdims=True)
    first_row = route_t[0:1, :].astype(jnp.float32)
    second_row = route_t[1:2, :].astype(jnp.float32)
    group_row = lax.shift_right_logical(route_t[0:1, :], GROUP_SIZE.bit_length() - 1).astype(jnp.float32)
    group_column = to_column(group_row)
    alike = jnp.broadcast_to(group_column, (rows, rows)) == spread_row(group_row)
    place_row = group_row * block + jnp.sum(jnp.where(alike & (i_row < i_col), 1.0, 0.0), 0, keepdims=True)
    place_column = to_column(place_row)
    perm_mask = spread_row(place_row) == i_row.astype(jnp.float32)
    perm = jnp.where(perm_mask, 1.0, 0.0).astype(jnp.bfloat16)
    back_mask = jnp.broadcast_to(place_column, (rows, rows)) == i_col.astype(jnp.float32)
    perm_back = jnp.where(back_mask, 1.0, 0.0).astype(jnp.bfloat16)
    first = jnp.sum(jnp.where(perm_mask, spread_row(first_row), 0.0), 1, keepdims=True)
    second = jnp.sum(jnp.where(perm_mask, spread_row(second_row), 0.0), 1, keepdims=True)
    hidden_sum = jnp.sum(dot32(perm, hid[...]), 1, keepdims=True)
    hidden_share = dot32(perm, hid[:, share_of(tp)])

    for load in w_loads:
        load.wait()
    for k in near_first:
        spreads[k].wait_recv()
    lhs = spread[...].reshape(n_ep * rows, depth)

    quad = GROUP_SIZE
    far_quads = range(1, n_ep // quad)
    bounds = [(0, cols), (cols, 2 * cols + DH), (2 * cols + DH, 3 * cols + DH), (3 * cols + DH, 4 * cols + DH)]
    cut = bounds[1][1]
    collected = [{} for _ in range(4)]
    arrivals = [{} for _ in range(4)]
    for i in range(4):
        part = dot32(lhs, weights[i])
        if i == 1:
            high, middle, low = three_parts(dot_t(lhs, gate_half))
            lane = lax.broadcasted_iota(jnp.int32, high.shape, 1)
            extra = jnp.where(lane < 2 * heads, high, jnp.where(lane < 4 * heads, middle, low))
            part = jnp.concatenate([part, extra], 1)
        span = slice(*bounds[i])
        proj_send[:, :, span] = part.astype(jnp.bfloat16).reshape(n_ep, rows, part.shape[1])
        proj_own[:, span] = part[:rows]
        for f in far_quads:
            far_own[f - 1, :, span] = part[f * quad * rows : (f * quad + 1) * rows]
        for f in far_quads:
            for j in range(quad - 1, 0, -1):
                collected[i][f, j] = begin(
                    remote(
                        proj_send.at[f * quad + j, :, span],
                        far_recv.at[f - 1, j - 1, :, span],
                        f_send.at[i, f - 1, j - 1],
                        f_recv.at[i, f - 1, j - 1],
                        (ep_peer[j], tp),
                    )
                )
    for i in range(4):
        span = slice(*bounds[i])
        for j in range(quad - 1, 0, -1):
            arrivals[i][j] = begin(
                remote(
                    proj_send.at[j, :, span], proj_recv.at[j, :, span], p_send.at[i, j], p_recv.at[i, j], (ep_peer[j], tp)
                )
            )
    crossed = [{} for _ in range(4)]
    for i in range(4):
        span = slice(*bounds[i])
        for f in far_quads:
            summed = far_own[f - 1, :, span]
            for j in range(1, quad):
                collected[i][f, j].wait_recv()
                summed += far_recv[f - 1, j - 1, :, span].astype(jnp.float32)
            if i < 2:
                source, target = cross_send.at[f - 1, :, span], cross_recv.at[f - 1, :, span]
                cross_send[f - 1, :, span] = summed
            else:
                span2 = slice(span.start - cut, span.stop - cut)
                source, target = cross_send2.at[f - 1, :, span2], cross_recv2.at[f - 1, :, span2]
                cross_send2[f - 1, :, span2] = summed.astype(jnp.bfloat16)
            crossed[i][f] = begin(
                remote(source, target, c_send.at[i, f - 1], c_recv.at[i, f - 1], (ep_peer[f * quad], tp))
            )

    def total(i):
        span = slice(*bounds[i])
        result = proj_own[:, span]
        for j in range(1, quad):
            arrivals[i][j].wait_recv()
            result += proj_recv[j, :, span].astype(jnp.float32)
        for f in far_quads:
            crossed[i][f].wait_recv()
            if i < 2:
                result += cross_recv[f - 1, :, span]
            else:
                result += cross_recv2[f - 1, :, span.start - cut : span.stop - cut].astype(jnp.float32)
        return result

    queries = total(0)
    read_old = []
    for h in range(heads):
        query = queries[:, h * DH : (h + 1) * DH]
        high = query.astype(jnp.bfloat16).astype(jnp.float32)
        both = jnp.concatenate([high, query - high], 0)
        row_of = lax.rem(lax.broadcasted_iota(jnp.int32, both.shape, 0), rows)
        spread_query = [jnp.where(row_of == b, both, 0.0).astype(jnp.bfloat16) for b in range(rows)]
        read = dot32(jnp.concatenate(spread_query, 1), mem_half[h])
        read_old.append(read[:rows] + read[rows:])
    second_total = total(1)
    keys = second_total[:, :cols] * DH ** (-0.5)
    gates = second_total[:, cols:]
    gates = gates + pltpu.roll(gates, DH - 2 * heads, 1) + pltpu.roll(gates, DH - 4 * heads, 1)
    scores = []
    for h in range(heads):
        span = slice(h * DH, (h + 1) * DH)
        scores.append(jnp.sum(queries[:, span] * keys[:, span], 1, keepdims=True))
    values = total(2)
    value_buf[...] = values
    last = total(3)
    mixed = []
    for h in range(heads):
        span = slice(h * DH, (h + 1) * DH)
        log_input = gates[:, h : h + 1] + input_bias[0:1, h : h + 1]
        forget = gates[:, heads + h : heads + h + 1] + forget_bias[0:1, h : h + 1]
        log_forget = jnp.minimum(forget, 0.0) - jnp.log1p(jnp.exp(-jnp.abs(forget)))
        carried = log_forget + to_column(max_state_t[h : h + 1, :])
        new_max = jnp.maximum(carried, log_input)
        keep = jnp.exp(carried - new_max)
        write = jnp.exp(log_input - new_max)
        max_out[h : h + 1, :] = to_row(new_max)
        keep_buf[h] = jnp.broadcast_to(keep, (rows, DH))
        write_keys[h * rows : (h + 1) * rows] = write * keys[:, span]
        readout = scores[h] * write * values[:, span] + keep * read_old[h]
        scaled = readout * lax.rsqrt(jnp.mean(readout * readout, -1, keepdims=True) + 1e-06)
        mixed.append((scaled * head_gain[:, span] * jax.nn.sigmoid(last[:, span])).astype(jnp.bfloat16))
    mixed_sorted = dot32(perm, jnp.concatenate(mixed, 1)).astype(jnp.bfloat16)

    out_load.wait()
    mixes = []
    partial_sum = jnp.zeros((rows, 1), jnp.float32)
    order = [o for o in range(1, n_tp)] + [0]
    for o in order:
        part = dot32(mixed_sorted, wo_buf[:, share_of(tp_peer[o])]).astype(jnp.bfloat16)
        mix_send[o] = part
        partial_sum += jnp.sum(part.astype(jnp.float32), 1, keepdims=True)
        if o:
            mixes.append(begin(remote(mix_send.at[o], mix_recv.at[o], m_send.at[o], m_recv.at[o], (me, tp_peer[o]))))
    high, middle, low = three_parts(partial_sum)
    lane = lax.broadcasted_iota(jnp.int32, (rows, DH), 1)
    parts = jnp.where(lane == 0, high, jnp.where(lane == 1, middle, jnp.where(lane == 2, low, 0.0)))
    sum_send[...] = parts.astype(jnp.bfloat16)
    sums = [
        begin(remote(sum_send, sum_recv.at[o], u_send.at[o], u_recv.at[o], (me, tp_peer[o]))) for o in range(1, n_tp)
    ]
    joined = res_alpha * hidden_share + mix_send[0].astype(jnp.float32)
    row_sum = res_alpha * hidden_sum + partial_sum
    for copy in mixes + sums:
        copy.wait_recv()
    for o in range(1, n_tp):
        joined += mix_recv[o].astype(jnp.float32)
        row_sum += jnp.sum(sum_recv[o].astype(jnp.float32), 1, keepdims=True)
    centred = joined - row_sum / width
    scaled_rows = centred * gain1[:, share_of(tp)]
    for g in range(groups):
        row_send[g] = scaled_rows[g * block : (g + 1) * block].astype(jnp.bfloat16)
    row_copies = {}
    for k in far_first + [0]:
        for j in range(n_y - 1, -1, -1):
            if k or j:
                row_copies[j, k] = begin(
                    remote(
                        row_send.at[lax.div(ep_peer[k], GROUP_SIZE)],
                        arrived.at[j, k],
                        a_send.at[j, k],
                        a_recv.at[j, k],
                        (ep_peer[k], 2 * y_peer[j] + core),
                    )
                )
    arrived[0, 0] = row_send[lax.div(me, GROUP_SIZE)]

    experts = expert_router_t.shape[0]
    expert_part = jnp.zeros((rows, experts), jnp.float32)
    group_part = jnp.zeros((rows, groups), jnp.float32)
    for piece in three_parts(scaled_rows):
        half = piece.astype(jnp.bfloat16)
        expert_part += dot_t(half, expert_router_t[:, share_of(tp)])
        group_part += dot_t(half, group_router_t[:, share_of(tp)])
    stat_send[...] = jnp.zeros_like(stat_send)
    stat_send[:, 0:experts] = expert_part
    stat_send[:, experts : experts + groups] = group_part
    stat_send[:, experts + groups : experts + groups + 1] = jnp.sum(centred * centred, 1, keepdims=True)
    stats = [
        begin(remote(stat_send, stat_recv.at[o], s_send.at[o], s_recv.at[o], (me, tp_peer[o]))) for o in range(1, n_tp)
    ]

    keys_t = write_keys[...].T
    for b in range(rows):
        for h in range(heads):
            old = mem_out[b, pl.ds(h, DH, stride=heads), :]
            column = keys_t[:, h * rows + b : h * rows + b + 1]
            value = value_buf[b : b + 1, h * DH : (h + 1) * DH]
            mem_out[b, pl.ds(h, DH, stride=heads), :] = keep_buf[h, b : b + 1, :] * old + column * value

    stat_total = stat_send[...]
    for o in range(1, n_tp):
        stats[o - 1].wait_recv()
        stat_total += stat_recv[o]
    row_scale = lax.rsqrt(stat_total[:, experts + groups : experts + groups + 1] / width + 1e-05)
    logits = stat_total * row_scale
    lanes = lax.broadcasted_iota(jnp.int32, logits.shape, 1).astype(jnp.float32)
    pick = lambda index: jnp.sum(jnp.where(lanes == index, logits, 0.0), 1, keepdims=True)
    first_logit = pick(first)
    second_logit = pick(second)
    group_gate = jax.nn.sigmoid(pick(experts + jnp.floor(first / GROUP_SIZE)))
    weight1 = group_gate * jax.nn.sigmoid(first_logit - second_logit)
    weight2 = group_gate * jax.nn.sigmoid(second_logit - first_logit)
    mid = (scaled_rows * row_scale).astype(jnp.bfloat16).astype(jnp.float32)
    for g in range(groups):
        span = slice(g * block, (g + 1) * block)
        for slot, column in enumerate((first, second, weight1, weight2)):
            weight_buf[slot, g] = jnp.broadcast_to(column[span], (block, DH))
        mid_buf[g] = res_alpha * mid[span]

    passed = {}
    for k in [0] + near_first:
        for j in range(n_y):
            if k or j:
                row_copies[j, k].wait_recv()
        passed[k] = begin(remote(arrived.at[:, k], arrived2.at[:, k], b_send.at[k], b_recv.at[k], partner))
    gate_load.wait()
    up_load.wait()
    count = n_ep * block
    gate_pre = jnp.zeros((count, wg_buf.shape[1]), jnp.float32)
    up_pre = jnp.zeros((count, wg_buf.shape[1]), jnp.float32)
    squares = jnp.zeros((count, DH), jnp.float32)
    for side, source in enumerate((arrived, arrived2)):
        if side:
            for k in range(n_ep):
                passed[k].wait_recv()
        for j in range(n_y):
            place = share_of(2 * y_from[j] + (1 - core if side else core))
            tokens32 = source[j].astype(jnp.float32).reshape(count, share)
            tokens = tokens32.astype(jnp.bfloat16)
            gate_pre += dot32(tokens, wg_buf[place, :])
            up_pre += dot32(tokens, wu_buf[place, :])
            plain = tokens32 / gain1[:, place]
            plain = plain * plain
            for c in range(share // DH):
                squares += plain[:, c * DH : (c + 1) * DH]
    token_scale = lax.rsqrt(jnp.sum(squares, 1, keepdims=True) / width + 1e-05)
    gate_pre *= token_scale
    units = (gate_pre * jax.nn.sigmoid(gate_pre) * (up_pre * token_scale)).astype(jnp.bfloat16)

    down_load.wait()
    downs = {}
    for j in range(n_y - 1, -1, -1):
        down_send[j] = dot32(units, wd_buf[:, share_of(2 * y_peer[j] + 1 - core)]).astype(jnp.bfloat16)
        downs[j] = begin(remote(down_send.at[j], down_recv.at[j], d_send.at[j], d_recv.at[j], partner))
    returns = {}
    own = {j: dot32(units, wd_buf[:, share_of(2 * y_peer[j] + core)]) for j in range(n_y - 1, -1, -1)}
    for j in range(n_y - 1, -1, -1):
        downs[j].wait_recv()
        result = own[j] + down_recv[j].astype(jnp.float32)
        for k in far_first + [0]:
            ret_send[j, k] = result[k * block : (k + 1) * block].astype(jnp.bfloat16)
            if k or j:
                returns[j, k] = begin(
                    remote(
                        ret_send.at[j, k],
                        ret_recv.at[j, k],
                        r_send.at[j, k],
                        r_recv.at[j, k],
                        (ep_peer[k], 2 * y_peer[j] + core),
                    )
                )
    for piece in range(groups):
        g = flip(lax.div(me, GROUP_SIZE), piece)
        gathered = mid_buf[g]
        for k in range(piece * GROUP_SIZE, (piece + 1) * GROUP_SIZE):
            expert = ep_peer[k].astype(jnp.float32)
            weight = jnp.where(weight_buf[0, g] == expert, weight_buf[2, g], 0.0)
            weight += jnp.where(weight_buf[1, g] == expert, weight_buf[3, g], 0.0)
            result = jnp.zeros((block, share), jnp.float32)
            for j in range(n_y):
                if k or j:
                    returns[j, k].wait_recv()
                result += (ret_recv[j, k] if k or j else ret_send[0, 0]).astype(jnp.float32)
            gathered += weight[:, 0:1] * result
        mid_buf[g] = gathered
    joined = mid_buf[...].reshape(rows, share)
    row_sum = jnp.sum(joined, -1, keepdims=True)
    square_sum = jnp.sum(joined * joined, -1, keepdims=True)
    stat2_send[...] = jnp.where(lane == 0, row_sum, square_sum)
    copies = [
        begin(remote(stat2_send, stat2_recv.at[o], t_send.at[o], t_recv.at[o], (me, tp_peer[o])))
        for o in range(1, n_tp)
    ]
    for o in range(1, n_tp):
        copies[o - 1].wait_recv()
        row_sum += stat2_recv[o][:, 0:1]
        square_sum += stat2_recv[o][:, 1:2]
    row_mean = row_sum / width
    row_var = square_sum / width - row_mean * row_mean
    result = ((joined - row_mean) * lax.rsqrt(row_var + 1e-05) * gain2[...]).astype(jnp.bfloat16)
    out_ref[...] = dot32(perm_back, result).astype(jnp.bfloat16)
    for copy in started:
        copy.wait_send()


def layer(n_ep, n_tp, groups, *operands):
    hidden, wq, _, _, _, memory, w_out, w_gate, _, w_down = operands[:10]
    rows, width = hidden.shape
    heads = memory.shape[1] // DH
    depth, cols = wq.shape
    share = width // n_tp
    block = rows // groups
    n_y = n_tp // 2
    half, full = jnp.bfloat16, jnp.float32
    vmem = pl.BlockSpec(memory_space=pltpu.VMEM)
    anywhere = pl.BlockSpec(memory_space=pl.ANY)
    dma = pltpu.SemaphoreType.DMA
    count = n_ep * block
    wide = 4 * cols + DH
    n_far = n_ep // GROUP_SIZE - 1
    return pl.pallas_call(
        functools.partial(layer_kernel, n_ep, n_tp, groups),
        out_shape=(
            pltpu.VMEM((rows, share), half),
            pltpu.VMEM(memory.shape, full),
            pltpu.VMEM((heads, rows), full),
        ),
        in_specs=[anywhere] * len(operands),
        out_specs=(vmem, vmem, vmem),
        scratch_shapes=[pltpu.VMEM(x.shape, x.dtype) for x in operands[10:]]
        + [
            pltpu.VMEM((rows, width), half),
            pltpu.VMEM((4, depth, cols), half),
            pltpu.VMEM(w_out.shape, half),
            pltpu.VMEM(w_gate.shape[1:], half),
            pltpu.VMEM(w_gate.shape[1:], half),
            pltpu.VMEM(w_down.shape[1:], half),
            pltpu.VMEM((heads, rows * DH, DH), half),
            pltpu.VMEM((DH, depth), full),
            pltpu.VMEM((n_ep, rows, depth), half),
            pltpu.VMEM((n_ep, rows, wide), half),
            pltpu.VMEM((n_ep, rows, wide), half),
            pltpu.VMEM((rows, wide), full),
            pltpu.VMEM((n_far, rows, wide), full),
            pltpu.VMEM((n_far, GROUP_SIZE - 1, rows, wide), half),
            pltpu.VMEM((n_far, rows, 2 * cols + DH), full),
            pltpu.VMEM((n_far, rows, 2 * cols + DH), full),
            pltpu.VMEM((n_far, rows, 2 * cols), half),
            pltpu.VMEM((n_far, rows, 2 * cols), half),
            pltpu.VMEM((heads * rows, DH), full),
            pltpu.VMEM((heads, rows, DH), full),
            pltpu.VMEM((rows, cols), full),
            pltpu.VMEM((n_tp, rows, share), half),
            pltpu.VMEM((n_tp, rows, share), half),
            pltpu.VMEM((rows, DH), half),
            pltpu.VMEM((n_tp, rows, DH), half),
            pltpu.VMEM((groups, block, share), half),
            pltpu.VMEM((n_y, n_ep, block, share), half),
            pltpu.VMEM((n_y, n_ep, block, share), half),
            pltpu.VMEM((rows, DH), full),
            pltpu.VMEM((n_tp, rows, DH), full),
            pltpu.VMEM((4, groups, block, DH), full),
            pltpu.VMEM((groups, block, share), full),
            pltpu.VMEM((n_y, count, share), half),
            pltpu.VMEM((n_y, count, share), half),
            pltpu.VMEM((n_y, n_ep, block, share), half),
            pltpu.VMEM((n_y, n_ep, block, share), half),
            pltpu.VMEM((rows, DH), full),
            pltpu.VMEM((n_tp, rows, DH), full),
            dma((10,)),
            dma((len(operands) - 10,)),
            dma((n_ep,)),
            dma((n_ep,)),
            dma((4, n_ep)),
            dma((4, n_ep)),
            dma((4, n_far, GROUP_SIZE - 1)),
            dma((4, n_far, GROUP_SIZE - 1)),
            dma((4, n_far)),
            dma((4, n_far)),
            dma((n_tp,)),
            dma((n_tp,)),
            dma((n_tp,)),
            dma((n_tp,)),
            dma((n_y, n_ep)),
            dma((n_y, n_ep)),
            dma((n_ep,)),
            dma((n_ep,)),
            dma((n_tp,)),
            dma((n_tp,)),
            dma((n_y,)),
            dma((n_y,)),
            dma((n_y, n_ep)),
            dma((n_y, n_ep)),
            dma((n_tp,)),
            dma((n_tp,)),
        ],
        compiler_params=pltpu.CompilerParams(
            collective_id=0, has_side_effects=True, vmem_limit_bytes=VMEM_LIMIT
        ),
        name="layer",
    )(*operands)


def store_kernel(result, memory, new_max, out_ref, mem_out, max_out, sems):
    copies = [
        pltpu.make_async_copy(source, target, sems.at[i])
        for i, (source, target) in enumerate(((memory, mem_out), (result, out_ref), (new_max, max_out)))
    ]
    for copy in copies:
        copy.start()
    for copy in copies:
        copy.wait()


def store(*operands):
    anywhere = pl.BlockSpec(memory_space=pl.ANY)
    return pl.pallas_call(
        store_kernel,
        out_shape=tuple(jax.ShapeDtypeStruct(x.shape, x.dtype) for x in operands),
        in_specs=[anywhere] * 3,
        out_specs=(anywhere,) * 3,
        scratch_shapes=[pltpu.SemaphoreType.DMA((3,))],
        compiler_params=pltpu.CompilerParams(vmem_limit_bytes=1 << 20),
        name="store",
    )(*operands)


def kernel_body(
    hidden_in,
    w_query,
    w_key,
    w_value,
    w_outgate,
    w_igate,
    w_fgate,
    input_bias,
    forget_bias,
    mem_state,
    max_state,
    head_gain,
    w_output,
    first_gain,
    w_group_router,
    w_expert_router,
    expert_route,
    w_expgate,
    w_expup,
    w_expdown,
    second_gain,
):
    n_ep, n_tp = lax.axis_size("ep"), lax.axis_size("tp")
    rows, heads, flat = mem_state.shape
    groups = w_group_router.shape[1]
    memory = mem_state.reshape(rows, heads, DH, DH).transpose(0, 2, 1, 3).reshape(rows, DH * heads, DH)
    results = layer(
        n_ep,
        n_tp,
        groups,
        hidden_in,
        w_query,
        w_key,
        w_value,
        w_outgate,
        memory,
        w_output,
        w_expgate,
        w_expup,
        w_expdown,
        w_igate.T,
        w_fgate.T,
        input_bias[None],
        forget_bias[None],
        max_state.T,
        head_gain[None],
        first_gain[None],
        second_gain[None],
        w_group_router.T,
        w_expert_router.T,
        expert_route.T,
    )
    hidden_out, memory_next, max_next = store(*results)
    memory_next = memory_next.reshape(rows, DH, heads, DH).transpose(0, 2, 1, 3).reshape(rows, heads, flat)
    return (hidden_out, memory_next, max_next.T)


def either_body(*operands):
    hidden_in, w_query, group_router, experts = operands[0], operands[1], operands[14], operands[17]
    rows, width = hidden_in.shape
    n_ep, n_tp = lax.axis_size("ep"), lax.axis_size("tp")
    groups = group_router.shape[1]
    block, odd_rows = divmod(rows, groups)
    aligned = rows % 16 == 0 and block % 8 == 0 and odd_rows == 0 and experts.shape[0] == 1
    aligned = aligned and w_query.shape[0] % DH == 0 and width // n_tp % DH == 0
    aligned = aligned and n_tp % 2 == 0 and n_ep & (n_ep - 1) == 0 and n_ep == groups * GROUP_SIZE and groups > 1
    return (kernel_body if aligned else body)(*operands)


def solution(mesh):
    return jax.shard_map(
        either_body,
        mesh=mesh,
        in_specs=(
            P("ep", None),
            P("ep", "tp"),
            P("ep", "tp"),
            P("ep", "tp"),
            P("ep", "tp"),
            P("ep", "tp"),
            P("ep", "tp"),
            P("tp"),
            P("tp"),
            P("ep", "tp", None),
            P("ep", "tp"),
            P("tp"),
            P("tp", None),
            P(),
            P(),
            P(),
            P("ep", None),
            P("ep", None, "tp"),
            P("ep", None, "tp"),
            P("ep", "tp", None),
            P("tp"),
        ),
        out_specs=(P("ep", "tp"), P("ep", "tp", None), P("ep", "tp")),
        check_vma=False,
    )
```

time: 95.7 us -> 51.1 us (0.53)
  Pallas kernels: 81.6 us -> 50.3 us
  local copies, waits for them, and re-layouts: 8.61 us -> 0 us
  other arithmetic: 4.08 us -> 0 us
    pallas_call x3 -> x2, Pallas kernels: 81.6 us -> 50.3 us  [the longest x1 48.3 us: layer(): pl.pallas_call(functools.partial(layer_kernel, n_ep, n_tp, groups), out_s...]
    unnamed x11 -> x0, local copies, waits for them, and re-layouts: 5.7 us -> none
    exp x2 -> x0, other arithmetic: 1.68 us -> none  [the longest x1 0.87 us: kernel_body(): write_new = jnp.exp(log_input - new_max)]
    broadcast_in_dim x2 -> x0, local copies, waits for them, and re-layouts: 1.39 us -> none  [kernel_body(): jnp.broadcast_to(gate[:, :, None], (rows, heads, DH))]
where the time goes in v1:
time: 51.1 us; the launch traced here: 51 us
  Pallas kernels  50.3 us (98%)
  between operations  0.65 us (1%)
    pallas_call x1, Pallas kernels, layer(): pl.pallas_call(functools.partial(layer_kernel, n_ep, n_tp, groups), out_s...  48.3 us
    pallas_call x1, Pallas kernels, store(): pl.pallas_call(store_kernel, out_shape=tuple((jax.ShapeDtypeStruct(x.shap...  2.05 us

profile of v1, /device:TPU:0, one launch (start us, length us, event | category | flops | bytes accessed | tf_op | source)
XLA Modules:
  0.0 51.0 jit_solution(11344354362149682419)
XLA Ops:
  0.6 48.3 %layer.1 = (bf16[16,1024]{1,0:T(8,128)(2,1)S(1)}, f32[16,512,128]{2,1,0:T(8,128)S(1)}, f32[4,16]{1,0:T(4,128)S(1)}) custom-call(bf16[16,4096]{1,0:T(8,128)(2,1)} %hidden_hbm.1, bf16[512,512]{1,0:T(8,128)(2,1)} %wq.1, bf16[512,512]{1,0:T(8,128)(2,1)} %wk.1, bf16[512,512]{1,0:T(8,128)(2,1)} %wv.1, bf16[512,512]{1,0:T(8,128)(2,1)} %wo.1, ...), custom_call_target="tpu_custom_call" | custom-call | tf_op jit(solution)/shard_map/layer/pallas_call | solution.py:736
  48.9 2.0 %store.1 = (bf16[16,1024]{1,0:T(8,128)(2,1)}, f32[16,512,128]{2,1,0:T(8,128)}, f32[4,16]{1,0:T(4,128)}) custom-call(bf16[16,1024]{1,0:T(8,128)(2,1)S(1)} %get-tuple-element.9.result, f32[16,512,128]{2,1,0:T(8,128)S(1)} %get-tuple-element.10.memory, f32[4,16]{1,0:T(4,128)S(1)} %get-tuple-element.11.new_max), custom_call_target="tpu_custom_call" | custom-call | tf_op jit(solution)/shard_map/store/pallas_call | solution.py:832

commit v2 on v1

--- a/solution.py
+++ b/solution.py
@@ -339,12 +339,12 @@
     y_from = [lax.rem(y + n_y - j, n_y) for j in range(n_y)]
     tp_peer = [lax.rem(tp + o, n_tp) for o in range(n_tp)]
     partner = (me, 2 * y + 1 - core)
-    started = []
-
-    def begin(copy):
-        copy.start()
-        started.append(copy)
-        return copy
+
+    def received(ref, sem):
+        remote(ref, ref, sem, sem, partner).wait_recv()
+
+    def sent(ref, sem):
+        remote(ref, ref, sem, sem, partner).wait_send()
 
     def share_of(index):
         return pl.ds(pl.multiple_of(index * share, share), share)
@@ -373,21 +373,20 @@
             )
         )
     ]
-    w_loads = [pltpu.make_async_copy(w, weights.at[i], load_sem.at[1 + i]) for i, w in enumerate((wq, wk, wv, wo))]
-    mem_load = pltpu.make_async_copy(memory, mem_out, load_sem.at[5])
-    out_load = pltpu.make_async_copy(w_out, wo_buf, load_sem.at[6])
-    gate_load = pltpu.make_async_copy(w_gate.at[0], wg_buf, load_sem.at[7])
-    up_load = pltpu.make_async_copy(w_up.at[0], wu_buf, load_sem.at[8])
-    down_load = pltpu.make_async_copy(w_down.at[0], wd_buf, load_sem.at[9])
+    w_loads = [pltpu.make_async_copy(w, weights.at[i], load_sem.at[1]) for i, w in enumerate((wq, wk, wv, wo))]
+    mem_load = pltpu.make_async_copy(memory, mem_out, load_sem.at[2])
+    out_load = pltpu.make_async_copy(w_out, wo_buf, load_sem.at[3])
+    gate_load = pltpu.make_async_copy(w_gate.at[0], wg_buf, load_sem.at[4])
+    up_load = pltpu.make_async_copy(w_up.at[0], wu_buf, load_sem.at[5])
+    down_load = pltpu.make_async_copy(w_down.at[0], wd_buf, load_sem.at[6])
     for load in small_loads + w_loads + [mem_load, out_load, gate_load, up_load, down_load]:
         load.start()
     hidden_load.wait()
     pl.semaphore_wait(barrier, len(peers))
 
-    spreads = {}
     for k in far_first:
         columns = pl.ds(pl.multiple_of(ep_peer[k] * depth, depth), depth)
-        spreads[k] = begin(remote(hid.at[:, columns], spread.at[k], h_send.at[k], h_recv.at[k], (ep_peer[k], tp)))
+        remote(hid.at[:, columns], spread.at[k], h_send.at[0], h_recv.at[0], (ep_peer[k], tp)).start()
     spread[0] = hid[:, pl.ds(pl.multiple_of(me * depth, depth), depth)]
     for load in small_loads:
         load.wait()
@@ -431,18 +430,14 @@
     hidden_sum = jnp.sum(dot32(perm, hid[...]), 1, keepdims=True)
     hidden_share = dot32(perm, hid[:, share_of(tp)])
 
-    for load in w_loads:
-        load.wait()
-    for k in near_first:
-        spreads[k].wait_recv()
+    pltpu.make_async_copy(weights, weights, load_sem.at[1]).wait()
+    received(spread.at[pl.ds(1, n_ep - 1)], h_recv.at[0])
     lhs = spread[...].reshape(n_ep * rows, depth)
 
     quad = GROUP_SIZE
     far_quads = range(1, n_ep // quad)
     bounds = [(0, cols), (cols, 2 * cols + DH), (2 * cols + DH, 3 * cols + DH), (3 * cols + DH, 4 * cols + DH)]
     cut = bounds[1][1]
-    collected = [{} for _ in range(4)]
-    arrivals = [{} for _ in range(4)]
     for i in range(4):
         part = dot32(lhs, weights[i])
         if i == 1:
@@ -457,30 +452,25 @@
             far_own[f - 1, :, span] = part[f * quad * rows : (f * quad + 1) * rows]
         for f in far_quads:
             for j in range(quad - 1, 0, -1):
-                collected[i][f, j] = begin(
-                    remote(
-                        proj_send.at[f * quad + j, :, span],
-                        far_recv.at[f - 1, j - 1, :, span],
-                        f_send.at[i, f - 1, j - 1],
-                        f_recv.at[i, f - 1, j - 1],
-                        (ep_peer[j], tp),
-                    )
-                )
+                remote(
+                    proj_send.at[f * quad + j, :, span],
+                    far_recv.at[f - 1, j - 1, :, span],
+                    f_send.at[0],
+                    f_recv.at[i],
+                    (ep_peer[j], tp),
+                ).start()
     for i in range(4):
         span = slice(*bounds[i])
         for j in range(quad - 1, 0, -1):
-            arrivals[i][j] = begin(
-                remote(
-                    proj_send.at[j, :, span], proj_recv.at[j, :, span], p_send.at[i, j], p_recv.at[i, j], (ep_peer[j], tp)
-                )
-            )
-    crossed = [{} for _ in range(4)]
+            remote(
+                proj_send.at[j, :, span], proj_recv.at[j, :, span], p_send.at[0], p_recv.at[i], (ep_peer[j], tp)
+            ).start()
     for i in range(4):
         span = slice(*bounds[i])
+        received(far_recv.at[:, :, :, span], f_recv.at[i])
         for f in far_quads:
             summed = far_own[f - 1, :, span]
             for j in range(1, quad):
-                collected[i][f, j].wait_recv()
                 summed += far_recv[f - 1, j - 1, :, span].astype(jnp.float32)
             if i < 2:
                 source, target = cross_send.at[f - 1, :, span], cross_recv.at[f - 1, :, span]
@@ -489,18 +479,19 @@
                 span2 = slice(span.start - cut, span.stop - cut)
                 source, target = cross_send2.at[f - 1, :, span2], cross_recv2.at[f - 1, :, span2]
                 cross_send2[f - 1, :, span2] = summed.astype(jnp.bfloat16)
-            crossed[i][f] = begin(
-                remote(source, target, c_send.at[i, f - 1], c_recv.at[i, f - 1], (ep_peer[f * quad], tp))
-            )
+            remote(source, target, c_send.at[i // 2], c_recv.at[i], (ep_peer[f * quad], tp)).start()
 
     def total(i):
         span = slice(*bounds[i])
         result = proj_own[:, span]
+        received(proj_recv.at[pl.ds(1, quad - 1), :, span], p_recv.at[i])
+        if i < 2:
+            received(cross_recv.at[:, :, span], c_recv.at[i])
+        else:
+            received(cross_recv2.at[:, :, slice(span.start - cut, span.stop - cut)], c_recv.at[i])
         for j in range(1, quad):
-            arrivals[i][j].wait_recv()
             result += proj_recv[j, :, span].astype(jnp.float32)
         for f in far_quads:
-            crossed[i][f].wait_recv()
             if i < 2:
                 result += cross_recv[f - 1, :, span]
             else:
@@ -547,7 +538,6 @@
     mixed_sorted = dot32(perm, jnp.concatenate(mixed, 1)).astype(jnp.bfloat16)
 
     out_load.wait()
-    mixes = []
     partial_sum = jnp.zeros((rows, 1), jnp.float32)
     order = [o for o in range(1, n_tp)] + [0]
     for o in order:
@@ -555,18 +545,18 @@
         mix_send[o] = part
         partial_sum += jnp.sum(part.astype(jnp.float32), 1, keepdims=True)
         if o:
-            mixes.append(begin(remote(mix_send.at[o], mix_recv.at[o], m_send.at[o], m_recv.at[o], (me, tp_peer[o]))))
+            remote(mix_send.at[o], mix_recv.at[o], m_send.at[0], m_recv.at[0], (me, tp_peer[o])).start()
     high, middle, low = three_parts(partial_sum)
     lane = lax.broadcasted_iota(jnp.int32, (rows, DH), 1)
     parts = jnp.where(lane == 0, high, jnp.where(lane == 1, middle, jnp.where(lane == 2, low, 0.0)))
     sum_send[...] = parts.astype(jnp.bfloat16)
-    sums = [
-        begin(remote(sum_send, sum_recv.at[o], u_send.at[o], u_recv.at[o], (me, tp_peer[o]))) for o in range(1, n_tp)
-    ]
+    others = pl.ds(1, n_tp - 1)
+    for o in range(1, n_tp):
+        remote(sum_send, sum_recv.at[o], u_send.at[0], u_recv.at[0], (me, tp_peer[o])).start()
     joined = res_alpha * hidden_share + mix_send[0].astype(jnp.float32)
     row_sum = res_alpha * hidden_sum + partial_sum
-    for copy in mixes + sums:
-        copy.wait_recv()
+    received(mix_recv.at[others], m_recv.at[0])
+    received(sum_recv.at[others], u_recv.at[0])
     for o in range(1, n_tp):
         joined += mix_recv[o].astype(jnp.float32)
         row_sum += jnp.sum(sum_recv[o].astype(jnp.float32), 1, keepdims=True)
@@ -574,19 +564,16 @@
     scaled_rows = centred * gain1[:, share_of(tp)]
     for g in range(groups):
         row_send[g] = scaled_rows[g * block : (g + 1) * block].astype(jnp.bfloat16)
-    row_copies = {}
     for k in far_first + [0]:
         for j in range(n_y - 1, -1, -1):
             if k or j:
-                row_copies[j, k] = begin(
-                    remote(
-                        row_send.at[lax.div(ep_peer[k], GROUP_SIZE)],
-                        arrived.at[j, k],
-                        a_send.at[j, k],
-                        a_recv.at[j, k],
-                        (ep_peer[k], 2 * y_peer[j] + core),
-                    )
-                )
+                remote(
+                    row_send.at[lax.div(ep_peer[k], GROUP_SIZE)],
+                    arrived.at[j, k],
+                    a_send.at[min(j, 1)],
+                    a_recv.at[k],
+                    (ep_peer[k], 2 * y_peer[j] + core),
+                ).start()
     arrived[0, 0] = row_send[lax.div(me, GROUP_SIZE)]
 
     experts = expert_router_t.shape[0]
@@ -600,9 +587,8 @@
     stat_send[:, 0:experts] = expert_part
     stat_send[:, experts : experts + groups] = group_part
     stat_send[:, experts + groups : experts + groups + 1] = jnp.sum(centred * centred, 1, keepdims=True)
-    stats = [
-        begin(remote(stat_send, stat_recv.at[o], s_send.at[o], s_recv.at[o], (me, tp_peer[o]))) for o in range(1, n_tp)
-    ]
+    for o in range(1, n_tp):
+        remote(stat_send, stat_recv.at[o], s_send.at[0], s_recv.at[0], (me, tp_peer[o])).start()
 
     keys_t = write_keys[...].T
     for b in range(rows):
@@ -613,8 +599,8 @@
             mem_out[b, pl.ds(h, DH, stride=heads), :] = keep_buf[h, b : b + 1, :] * old + column * value
 
     stat_total = stat_send[...]
+    received(stat_recv.at[others], s_recv.at[0])
     for o in range(1, n_tp):
-        stats[o - 1].wait_recv()
         stat_total += stat_recv[o]
     row_scale = lax.rsqrt(stat_total[:, experts + groups : experts + groups + 1] / width + 1e-05)
     logits = stat_total * row_scale
@@ -632,12 +618,10 @@
             weight_buf[slot, g] = jnp.broadcast_to(column[span], (block, DH))
         mid_buf[g] = res_alpha * mid[span]
 
-    passed = {}
     for k in [0] + near_first:
-        for j in range(n_y):
-            if k or j:
-                row_copies[j, k].wait_recv()
-        passed[k] = begin(remote(arrived.at[:, k], arrived2.at[:, k], b_send.at[k], b_recv.at[k], partner))
+        first_j = 0 if k else 1
+        received(arrived.at[pl.ds(first_j, n_y - first_j), k], a_recv.at[k])
+        remote(arrived.at[:, k], arrived2.at[:, k], b_send.at[0], b_recv.at[0], partner).start()
     gate_load.wait()
     up_load.wait()
     count = n_ep * block
@@ -646,8 +630,7 @@
     squares = jnp.zeros((count, DH), jnp.float32)
     for side, source in enumerate((arrived, arrived2)):
         if side:
-            for k in range(n_ep):
-                passed[k].wait_recv()
+            received(arrived2, b_recv.at[0])
         for j in range(n_y):
             place = share_of(2 * y_from[j] + (1 - core if side else core))
             tokens32 = source[j].astype(jnp.float32).reshape(count, share)
@@ -663,27 +646,23 @@
     units = (gate_pre * jax.nn.sigmoid(gate_pre) * (up_pre * token_scale)).astype(jnp.bfloat16)
 
     down_load.wait()
-    downs = {}
     for j in range(n_y - 1, -1, -1):
         down_send[j] = dot32(units, wd_buf[:, share_of(2 * y_peer[j] + 1 - core)]).astype(jnp.bfloat16)
-        downs[j] = begin(remote(down_send.at[j], down_recv.at[j], d_send.at[j], d_recv.at[j], partner))
-    returns = {}
+        remote(down_send.at[j], down_recv.at[j], d_send.at[0], d_recv.at[j], partner).start()
     own = {j: dot32(units, wd_buf[:, share_of(2 * y_peer[j] + core)]) for j in range(n_y - 1, -1, -1)}
     for j in range(n_y - 1, -1, -1):
-        downs[j].wait_recv()
+        received(down_recv.at[j], d_recv.at[j])
         result = own[j] + down_recv[j].astype(jnp.float32)
         for k in far_first + [0]:
             ret_send[j, k] = result[k * block : (k + 1) * block].astype(jnp.bfloat16)
             if k or j:
-                returns[j, k] = begin(
-                    remote(
-                        ret_send.at[j, k],
-                        ret_recv.at[j, k],
-                        r_send.at[j, k],
-                        r_recv.at[j, k],
-                        (ep_peer[k], 2 * y_peer[j] + core),
-                    )
-                )
+                remote(
+                    ret_send.at[j, k],
+                    ret_recv.at[j, k],
+                    r_send.at[min(j, 1)],
+                    r_recv.at[k],
+                    (ep_peer[k], 2 * y_peer[j] + core),
+                ).start()
     for piece in range(groups):
         g = flip(lax.div(me, GROUP_SIZE), piece)
         gathered = mid_buf[g]
@@ -691,10 +670,10 @@
             expert = ep_peer[k].astype(jnp.float32)
             weight = jnp.where(weight_buf[0, g] == expert, weight_buf[2, g], 0.0)
             weight += jnp.where(weight_buf[1, g] == expert, weight_buf[3, g], 0.0)
+            first_j = 0 if k else 1
+            received(ret_recv.at[pl.ds(first_j, n_y - first_j), k], r_recv.at[k])
             result = jnp.zeros((block, share), jnp.float32)
             for j in range(n_y):
-                if k or j:
-                    returns[j, k].wait_recv()
                 result += (ret_recv[j, k] if k or j else ret_send[0, 0]).astype(jnp.float32)
             gathered += weight[:, 0:1] * result
         mid_buf[g] = gathered
@@ -702,20 +681,35 @@
     row_sum = jnp.sum(joined, -1, keepdims=True)
     square_sum = jnp.sum(joined * joined, -1, keepdims=True)
     stat2_send[...] = jnp.where(lane == 0, row_sum, square_sum)
-    copies = [
-        begin(remote(stat2_send, stat2_recv.at[o], t_send.at[o], t_recv.at[o], (me, tp_peer[o])))
-        for o in range(1, n_tp)
-    ]
     for o in range(1, n_tp):
-        copies[o - 1].wait_recv()
+        remote(stat2_send, stat2_recv.at[o], t_send.at[0], t_recv.at[0], (me, tp_peer[o])).start()
+    received(stat2_recv.at[others], t_recv.at[0])
+    for o in range(1, n_tp):
         row_sum += stat2_recv[o][:, 0:1]
         square_sum += stat2_recv[o][:, 1:2]
     row_mean = row_sum / width
     row_var = square_sum / width - row_mean * row_mean
     result = ((joined - row_mean) * lax.rsqrt(row_var + 1e-05) * gain2[...]).astype(jnp.bfloat16)
     out_ref[...] = dot32(perm_back, result).astype(jnp.bfloat16)
-    for copy in started:
-        copy.wait_send()
+    rest = pl.ds(1, n_ep - 1)
+    for ref, sem in (
+        (spread.at[rest], h_send.at[0]),
+        (far_recv, f_send.at[0]),
+        (proj_recv.at[pl.ds(1, quad - 1)], p_send.at[0]),
+        (cross_send, c_send.at[0]),
+        (cross_send2, c_send.at[1]),
+        (mix_send.at[others], m_send.at[0]),
+        (sum_recv.at[others], u_send.at[0]),
+        (arrived.at[0, rest], a_send.at[0]),
+        (arrived.at[pl.ds(1, n_y - 1)], a_send.at[1]),
+        (stat_recv.at[others], s_send.at[0]),
+        (arrived, b_send.at[0]),
+        (down_send, d_send.at[0]),
+        (ret_send.at[0, rest], r_send.at[0]),
+        (ret_send.at[pl.ds(1, n_y - 1)], r_send.at[1]),
+        (stat2_recv.at[others], t_send.at[0]),
+    ):
+        sent(ref, sem)
 
 
 def layer(n_ep, n_tp, groups, *operands):
@@ -782,32 +776,32 @@
             pltpu.VMEM((n_y, n_ep, block, share), half),
             pltpu.VMEM((rows, DH), full),
             pltpu.VMEM((n_tp, rows, DH), full),
-            dma((10,)),
+            dma((7,)),
             dma((len(operands) - 10,)),
+            dma((1,)),
+            dma((1,)),
+            dma((1,)),
+            dma((4,)),
+            dma((1,)),
+            dma((4,)),
+            dma((2,)),
+            dma((4,)),
+            dma((1,)),
+            dma((1,)),
+            dma((1,)),
+            dma((1,)),
+            dma((2,)),
             dma((n_ep,)),
+            dma((1,)),
+            dma((1,)),
+            dma((1,)),
+            dma((1,)),
+            dma((1,)),
+            dma((n_y,)),
+            dma((2,)),
             dma((n_ep,)),
-            dma((4, n_ep)),
-            dma((4, n_ep)),
-            dma((4, n_far, GROUP_SIZE - 1)),
-            dma((4, n_far, GROUP_SIZE - 1)),
-            dma((4, n_far)),
-            dma((4, n_far)),
-            dma((n_tp,)),
-            dma((n_tp,)),
-            dma((n_tp,)),
-            dma((n_tp,)),
-            dma((n_y, n_ep)),
-            dma((n_y, n_ep)),
-            dma((n_ep,)),
-            dma((n_ep,)),
-            dma((n_tp,)),
-            dma((n_tp,)),
-            dma((n_y,)),
-            dma((n_y,)),
-            dma((n_y, n_ep)),
-            dma((n_y, n_ep)),
-            dma((n_tp,)),
-            dma((n_tp,)),
+            dma((1,)),
+            dma((1,)),
         ],
         compiler_params=pltpu.CompilerParams(
             collective_id=0, has_side_effects=True, vmem_limit_bytes=VMEM_LIMIT

time: 51.1 us -> 49.4 us (0.967)
  Pallas kernels: 50.3 us -> 48.6 us
    pallas_call x1, Pallas kernels: 48.3 us -> 46.5 us  [layer(): pl.pallas_call(functools.partial(layer_kernel, n_ep, n_tp, groups), out_s...]
where the time goes in v2:
time: 49.4 us; the launch traced here: 49.2 us
  Pallas kernels  48.6 us (98%)
  between operations  0.65 us (1%)
    pallas_call x1, Pallas kernels, layer(): pl.pallas_call(functools.partial(layer_kernel, n_ep, n_tp, groups), out_s...  46.5 us
    pallas_call x1, Pallas kernels, store(): pl.pallas_call(store_kernel, out_shape=tuple((jax.ShapeDtypeStruct(x.shap...  2.05 us

profile of v2, /device:TPU:0, one launch (start us, length us, event | category | flops | bytes accessed | tf_op | source)
XLA Modules:
  0.0 49.2 jit_solution(10996161884380823722)
XLA Ops:
  0.6 46.5 %layer.1 = (bf16[16,1024]{1,0:T(8,128)(2,1)S(1)}, f32[16,512,128]{2,1,0:T(8,128)S(1)}, f32[4,16]{1,0:T(4,128)S(1)}) custom-call(bf16[16,4096]{1,0:T(8,128)(2,1)} %hidden_hbm.1, bf16[512,512]{1,0:T(8,128)(2,1)} %wq.1, bf16[512,512]{1,0:T(8,128)(2,1)} %wk.1, bf16[512,512]{1,0:T(8,128)(2,1)} %wv.1, bf16[512,512]{1,0:T(8,128)(2,1)} %wo.1, ...), custom_call_target="tpu_custom_call" | custom-call | tf_op jit(solution)/shard_map/layer/pallas_call | solution.py:730
  47.2 2.0 %store.1 = (bf16[16,1024]{1,0:T(8,128)(2,1)}, f32[16,512,128]{2,1,0:T(8,128)}, f32[4,16]{1,0:T(4,128)}) custom-call(bf16[16,1024]{1,0:T(8,128)(2,1)S(1)} %get-tuple-element.9.result, f32[16,512,128]{2,1,0:T(8,128)S(1)} %get-tuple-element.10.memory, f32[4,16]{1,0:T(4,128)S(1)} %get-tuple-element.11.new_max), custom_call_target="tpu_custom_call" | custom-call | tf_op jit(solution)/shard_map/store/pallas_call | solution.py:826

commit v3 on v2

--- a/solution.py
+++ b/solution.py
@@ -284,13 +284,17 @@
     sum_recv,
     row_send,
     arrived,
-    arrived2,
+    square_send,
+    square_recv,
     stat_send,
     stat_recv,
     weight_buf,
     mid_buf,
-    down_send,
-    down_recv,
+    part_send,
+    part_recv,
+    wg_other,
+    wu_other,
+    wd_other,
     ret_send,
     ret_recv,
     stat2_send,
@@ -317,6 +321,8 @@
     s_recv,
     d_send,
     d_recv,
+    w_send,
+    w_recv,
     r_send,
     r_recv,
     t_send,
@@ -481,6 +487,16 @@
                 cross_send2[f - 1, :, span2] = summed.astype(jnp.bfloat16)
             remote(source, target, c_send.at[i // 2], c_recv.at[i], (ep_peer[f * quad], tp)).start()
 
+    down_load.wait()
+    gate_load.wait()
+    up_load.wait()
+    for j in range(n_y):
+        place = share_of(2 * y_from[j] + 1 - core)
+        remote(wg_buf.at[place], wg_other.at[j], w_send.at[0], w_recv.at[0], partner).start()
+        remote(wu_buf.at[place], wu_other.at[j], w_send.at[1], w_recv.at[1], partner).start()
+        theirs = wd_buf.at[:, share_of(2 * y_peer[j] + 1 - core)]
+        remote(theirs, wd_other.at[j], w_send.at[2], w_recv.at[2], partner).start()
+
     def total(i):
         span = slice(*bounds[i])
         result = proj_own[:, span]
@@ -618,43 +634,52 @@
             weight_buf[slot, g] = jnp.broadcast_to(column[span], (block, DH))
         mid_buf[g] = res_alpha * mid[span]
 
+    received(wg_other, w_recv.at[0])
+    received(wu_other, w_recv.at[1])
+    received(wd_other, w_recv.at[2])
     for k in [0] + near_first:
         first_j = 0 if k else 1
         received(arrived.at[pl.ds(first_j, n_y - first_j), k], a_recv.at[k])
-        remote(arrived.at[:, k], arrived2.at[:, k], b_send.at[0], b_recv.at[0], partner).start()
-    gate_load.wait()
-    up_load.wait()
     count = n_ep * block
-    gate_pre = jnp.zeros((count, wg_buf.shape[1]), jnp.float32)
-    up_pre = jnp.zeros((count, wg_buf.shape[1]), jnp.float32)
+    hidden_units = wg_buf.shape[1]
+    tokens32 = [arrived[j].astype(jnp.float32).reshape(count, share) for j in range(n_y)]
+    tokens = [token.astype(jnp.bfloat16) for token in tokens32]
+    places = [share_of(2 * y_from[j] + core) for j in range(n_y)]
     squares = jnp.zeros((count, DH), jnp.float32)
-    for side, source in enumerate((arrived, arrived2)):
-        if side:
-            received(arrived2, b_recv.at[0])
+    for j in range(n_y):
+        plain = tokens32[j] / gain1[:, places[j]]
+        plain = plain * plain
+        for c in range(share // DH):
+            squares += plain[:, c * DH : (c + 1) * DH]
+    square_send[...] = squares
+    remote(square_send, square_recv, b_send.at[0], b_recv.at[0], partner).start()
+    partial = []
+    for side in range(2):
+        gate_pre = jnp.zeros((count, hidden_units), jnp.float32)
+        up_pre = jnp.zeros((count, hidden_units), jnp.float32)
         for j in range(n_y):
-            place = share_of(2 * y_from[j] + (1 - core if side else core))
-            tokens32 = source[j].astype(jnp.float32).reshape(count, share)
-            tokens = tokens32.astype(jnp.bfloat16)
-            gate_pre += dot32(tokens, wg_buf[place, :])
-            up_pre += dot32(tokens, wu_buf[place, :])
-            plain = tokens32 / gain1[:, place]
-            plain = plain * plain
-            for c in range(share // DH):
-                squares += plain[:, c * DH : (c + 1) * DH]
+            gate_pre += dot32(tokens[j], wg_other[j] if side else wg_buf[places[j], :])
+            up_pre += dot32(tokens[j], wu_other[j] if side else wu_buf[places[j], :])
+        partial.append((gate_pre, up_pre))
+        part_send[side, :, 0:hidden_units] = gate_pre.astype(jnp.bfloat16)
+        part_send[side, :, hidden_units:] = up_pre.astype(jnp.bfloat16)
+        remote(part_send.at[side], part_recv.at[side], d_send.at[0], d_recv.at[0], partner).start()
+    received(square_recv, b_recv.at[0])
+    squares += square_recv[...]
     token_scale = lax.rsqrt(jnp.sum(squares, 1, keepdims=True) / width + 1e-05)
-    gate_pre *= token_scale
-    units = (gate_pre * jax.nn.sigmoid(gate_pre) * (up_pre * token_scale)).astype(jnp.bfloat16)
-
-    down_load.wait()
+    received(part_recv, d_recv.at[0])
+    units = []
+    for side in range(2):
+        gate_pre = (partial[side][0] + part_recv[1 - side, :, 0:hidden_units].astype(jnp.float32)) * token_scale
+        up_pre = (partial[side][1] + part_recv[1 - side, :, hidden_units:].astype(jnp.float32)) * token_scale
+        units.append((gate_pre * jax.nn.sigmoid(gate_pre) * up_pre).astype(jnp.bfloat16))
+
     for j in range(n_y - 1, -1, -1):
-        down_send[j] = dot32(units, wd_buf[:, share_of(2 * y_peer[j] + 1 - core)]).astype(jnp.bfloat16)
-        remote(down_send.at[j], down_recv.at[j], d_send.at[0], d_recv.at[j], partner).start()
-    own = {j: dot32(units, wd_buf[:, share_of(2 * y_peer[j] + core)]) for j in range(n_y - 1, -1, -1)}
-    for j in range(n_y - 1, -1, -1):
-        received(down_recv.at[j], d_recv.at[j])
-        result = own[j] + down_recv[j].astype(jnp.float32)
-        for k in far_first + [0]:
+        result = dot32(units[0], wd_buf[:, share_of(2 * y_peer[j] + core)]) + dot32(units[1], wd_other[j])
+        for k in range(n_ep):
             ret_send[j, k] = result[k * block : (k + 1) * block].astype(jnp.bfloat16)
+    for k in far_first + [0]:
+        for j in range(n_y - 1, -1, -1):
             if k or j:
                 remote(
                     ret_send.at[j, k],
@@ -703,8 +728,11 @@
         (arrived.at[0, rest], a_send.at[0]),
         (arrived.at[pl.ds(1, n_y - 1)], a_send.at[1]),
         (stat_recv.at[others], s_send.at[0]),
-        (arrived, b_send.at[0]),
-        (down_send, d_send.at[0]),
+        (square_send, b_send.at[0]),
+        (part_send, d_send.at[0]),
+        (wg_other, w_send.at[0]),
+        (wu_other, w_send.at[1]),
+        (wd_other, w_send.at[2]),
         (ret_send.at[0, rest], r_send.at[0]),
         (ret_send.at[pl.ds(1, n_y - 1)], r_send.at[1]),
         (stat2_recv.at[others], t_send.at[0]),
@@ -765,13 +793,17 @@
             pltpu.VMEM((n_tp, rows, DH), half),
             pltpu.VMEM((groups, block, share), half),
             pltpu.VMEM((n_y, n_ep, block, share), half),
-            pltpu.VMEM((n_y, n_ep, block, share), half),
+            pltpu.VMEM((count, DH), full),
+            pltpu.VMEM((count, DH), full),
             pltpu.VMEM((rows, DH), full),
             pltpu.VMEM((n_tp, rows, DH), full),
             pltpu.VMEM((4, groups, block, DH), full),
             pltpu.VMEM((groups, block, share), full),
-            pltpu.VMEM((n_y, count, share), half),
-            pltpu.VMEM((n_y, count, share), half),
+            pltpu.VMEM((2, count, 2 * w_gate.shape[2]), half),
+            pltpu.VMEM((2, count, 2 * w_gate.shape[2]), half),
+            pltpu.VMEM((n_y, share, w_gate.shape[2]), half),
+            pltpu.VMEM((n_y, share, w_gate.shape[2]), half),
+            pltpu.VMEM((n_y, w_down.shape[1], share), half),
             pltpu.VMEM((n_y, n_ep, block, share), half),
             pltpu.VMEM((n_y, n_ep, block, share), half),
             pltpu.VMEM((rows, DH), full),
@@ -797,7 +829,9 @@
             dma((1,)),
             dma((1,)),
             dma((1,)),
-            dma((n_y,)),
+            dma((1,)),
+            dma((3,)),
+            dma((3,)),
             dma((2,)),
             dma((n_ep,)),
             dma((1,)),

time: 49.4 us -> 48.9 us (0.990)
  Pallas kernels: 48.6 us -> 48.1 us
    pallas_call x1, Pallas kernels: 46.5 us -> 46 us  [layer(): pl.pallas_call(functools.partial(layer_kernel, n_ep, n_tp, groups), out_s...]
where the time goes in v3:
time: 48.9 us; the launch traced here: 48.7 us
  Pallas kernels  48.1 us (98%)
  between operations  0.65 us (1%)
    pallas_call x1, Pallas kernels, layer(): pl.pallas_call(functools.partial(layer_kernel, n_ep, n_tp, groups), out_s...  46 us
    pallas_call x1, Pallas kernels, store(): pl.pallas_call(store_kernel, out_shape=tuple((jax.ShapeDtypeStruct(x.shap...  2.05 us

profile of v3, /device:TPU:0, one launch (start us, length us, event | category | flops | bytes accessed | tf_op | source)
XLA Modules:
  0.0 48.7 jit_solution(11240927819299890429)
XLA Ops:
  0.6 46.0 %layer.1 = (bf16[16,1024]{1,0:T(8,128)(2,1)S(1)}, f32[16,512,128]{2,1,0:T(8,128)S(1)}, f32[4,16]{1,0:T(4,128)S(1)}) custom-call(bf16[16,4096]{1,0:T(8,128)(2,1)} %hidden_hbm.1, bf16[512,512]{1,0:T(8,128)(2,1)} %wq.1, bf16[512,512]{1,0:T(8,128)(2,1)} %wk.1, bf16[512,512]{1,0:T(8,128)(2,1)} %wv.1, bf16[512,512]{1,0:T(8,128)(2,1)} %wo.1, ...), custom_call_target="tpu_custom_call" | custom-call | tf_op jit(solution)/shard_map/layer/pallas_call | solution.py:758
  46.7 2.0 %store.1 = (bf16[16,1024]{1,0:T(8,128)(2,1)}, f32[16,512,128]{2,1,0:T(8,128)}, f32[4,16]{1,0:T(4,128)}) custom-call(bf16[16,1024]{1,0:T(8,128)(2,1)S(1)} %get-tuple-element.9.result, f32[16,512,128]{2,1,0:T(8,128)S(1)} %get-tuple-element.10.memory, f32[4,16]{1,0:T(4,128)S(1)} %get-tuple-element.11.new_max), custom_call_target="tpu_custom_call" | custom-call | tf_op jit(solution)/shard_map/store/pallas_call | solution.py:860

commit v4 on v3

--- a/solution.py
+++ b/solution.py
@@ -300,7 +300,6 @@
     stat2_send,
     stat2_recv,
     load_sem,
-    small_sem,
     h_send,
     h_recv,
     p_send,
@@ -343,7 +342,7 @@
     ep_peer = [flip(me, k) for k in range(n_ep)]
     y_peer = [lax.rem(y + j, n_y) for j in range(n_y)]
     y_from = [lax.rem(y + n_y - j, n_y) for j in range(n_y)]
-    tp_peer = [lax.rem(tp + o, n_tp) for o in range(n_tp)]
+    tp_peer = [flip(tp, o) for o in range(n_tp)]
     partner = (me, 2 * y + 1 - core)
 
     def received(ref, sem):
@@ -362,8 +361,9 @@
     hidden_load = pltpu.make_async_copy(hidden_hbm, hid, load_sem.at[0])
     hidden_load.start()
     small_loads = [
-        pltpu.make_async_copy(source, target, small_sem.at[i])
-        for i, (source, target) in enumerate(
+        pltpu.make_async_copy(source, target, sem)
+        for sem, (source, target) in zip(
+            (p_send.at[0], f_send.at[0], c_send.at[0], c_send.at[1], m_send.at[0], u_send.at[0], a_send.at[0], a_send.at[1], b_send.at[0], s_send.at[0], d_send.at[0]),
             (
                 (w_igate_t_hbm, w_igate_t),
                 (w_fgate_t_hbm, w_fgate_t),
@@ -555,7 +555,7 @@
 
     out_load.wait()
     partial_sum = jnp.zeros((rows, 1), jnp.float32)
-    order = [o for o in range(1, n_tp)] + [0]
+    order = list(range(n_tp - 1, -1, -1))
     for o in order:
         part = dot32(mixed_sorted, wo_buf[:, share_of(tp_peer[o])]).astype(jnp.bfloat16)
         mix_send[o] = part
@@ -676,10 +676,9 @@
 
     for j in range(n_y - 1, -1, -1):
         result = dot32(units[0], wd_buf[:, share_of(2 * y_peer[j] + core)]) + dot32(units[1], wd_other[j])
-        for k in range(n_ep):
+        for k in far_first + [0]:
             ret_send[j, k] = result[k * block : (k + 1) * block].astype(jnp.bfloat16)
-    for k in far_first + [0]:
-        for j in range(n_y - 1, -1, -1):
+        for k in far_first + [0]:
             if k or j:
                 remote(
                     ret_send.at[j, k],
@@ -809,7 +808,6 @@
             pltpu.VMEM((rows, DH), full),
             pltpu.VMEM((n_tp, rows, DH), full),
             dma((7,)),
-            dma((len(operands) - 10,)),
             dma((1,)),
             dma((1,)),
             dma((1,)),
@@ -934,7 +932,7 @@
     block, odd_rows = divmod(rows, groups)
     aligned = rows % 16 == 0 and block % 8 == 0 and odd_rows == 0 and experts.shape[0] == 1
     aligned = aligned and w_query.shape[0] % DH == 0 and width // n_tp % DH == 0
-    aligned = aligned and n_tp % 2 == 0 and n_ep & (n_ep - 1) == 0 and n_ep == groups * GROUP_SIZE and groups > 1
+    aligned = aligned and n_tp % 2 == 0 and n_tp & (n_tp - 1) == 0 and n_ep & (n_ep - 1) == 0 and n_ep == groups * GROUP_SIZE and groups > 1
     return (kernel_body if aligned else body)(*operands)
 
 

time: 48.9 us -> 47.8 us (0.978)
  Pallas kernels: 48.1 us -> 47 us
    pallas_call x1, Pallas kernels: 46 us -> 44.9 us  [layer(): pl.pallas_call(functools.partial(layer_kernel, n_ep, n_tp, groups), out_s...]
where the time goes in v4:
time: 47.8 us; the launch traced here: 47.6 us
  Pallas kernels  47 us (98%)
  between operations  0.65 us (1%)
    pallas_call x1, Pallas kernels, layer(): pl.pallas_call(functools.partial(layer_kernel, n_ep, n_tp, groups), out_s...  44.9 us
    pallas_call x1, Pallas kernels, store(): pl.pallas_call(store_kernel, out_shape=tuple((jax.ShapeDtypeStruct(x.shap...  2.05 us

profile of v4, /device:TPU:0, one launch (start us, length us, event | category | flops | bytes accessed | tf_op | source)
XLA Modules:
  0.0 47.6 jit_solution(4053329578471162888)
XLA Ops:
  0.6 44.9 %layer.1 = (bf16[16,1024]{1,0:T(8,128)(2,1)S(1)}, f32[16,512,128]{2,1,0:T(8,128)S(1)}, f32[4,16]{1,0:T(4,128)S(1)}) custom-call(bf16[16,4096]{1,0:T(8,128)(2,1)} %hidden_hbm.1, bf16[512,512]{1,0:T(8,128)(2,1)} %wq.1, bf16[512,512]{1,0:T(8,128)(2,1)} %wk.1, bf16[512,512]{1,0:T(8,128)(2,1)} %wv.1, bf16[512,512]{1,0:T(8,128)(2,1)} %wo.1, ...), custom_call_target="tpu_custom_call" | custom-call | tf_op jit(solution)/shard_map/layer/pallas_call | solution.py:757
  45.6 2.0 %store.1 = (bf16[16,1024]{1,0:T(8,128)(2,1)}, f32[16,512,128]{2,1,0:T(8,128)}, f32[4,16]{1,0:T(4,128)}) custom-call(bf16[16,1024]{1,0:T(8,128)(2,1)S(1)} %get-tuple-element.9.result, f32[16,512,128]{2,1,0:T(8,128)S(1)} %get-tuple-element.10.memory, f32[4,16]{1,0:T(4,128)S(1)} %get-tuple-element.11.new_max), custom_call_target="tpu_custom_call" | custom-call | tf_op jit(solution)/shard_map/store/pallas_call | solution.py:858
